TPU v7x, 256 devices: a whole 4x4x8 slice. The times are simulated.
256 devices in a mesh: sp: 16 (over y, x), tp: 16 (over z, core).
Axes of the slice: x: 4, y: 4, z: 8, core: 2. Of those that a mesh axis runs over, the one named last changes fastest.
Arguments:
- queries: bfloat16 [6144, 2048], P('sp', 'tp'), may hold values from -6 to 6
- keys: bfloat16 [6144, 2048], P('sp', 'tp'), may hold values from -6 to 6
- values: bfloat16 [6144, 2048], P('sp', 'tp'), may hold values from -6 to 6
- key_bias: bfloat16 [6144, 32], P('sp', 'tp'), may hold values from -16 to 0
- head_gain: float32 [32, 64], P('tp'), may hold values from 0.1 to 1.9
- out_weight: bfloat16 [2048, 2048], P('tp'), may hold values from -0.125 to 0.125
- residual: bfloat16 [6144, 2048], P(('sp', 'tp')), may hold values from -6 to 6
- norm_gain: float32 [2048], replicated, may hold values from 0.1 to 1.9
- gate_proj: bfloat16 [16, 2048, 7168], P('sp', None, 'tp'), may hold values from -0.125 to 0.125
- up_proj: bfloat16 [16, 2048, 7168], P('sp', None, 'tp'), may hold values from -0.125 to 0.125
- down_proj: bfloat16 [16, 7168, 2048], P('sp', 'tp'), may hold values from -0.0625 to 0.0625
- expert_choice: int32 [6144, 2], P(('sp', 'tp')), may hold values from 0 to 15, all different within a row; in each aligned block of 24 rows (0 to 23, 24 to 47, ...) at most 6 rows name the same one
- expert_weights: float32 [6144, 2], P(('sp', 'tp')), may hold values from 0.2 to 1
Outputs:
- layer_out: bfloat16 [6144, 2048], P(('sp', 'tp'))
Inputs may be any that keep to these rules, and one draw needn't show every extreme that they name: `expert_choice`: in each aligned block of 24 rows (the rows of one device), no expert is named more than 6 times; the two experts of a row differ.
All inputs are finite; a program needn't handle non-finite values.
Results may differ from a plain program's by a relative error of at most 0.019.
Values may be sent and summed in bfloat16 or wider, within the bound.
A program may use at most 128 MiB of HBM per device.

v0:
```python
import jax
import jax.numpy as jnp
from jax import lax
from jax.sharding import PartitionSpec as P

epsilon = 1e-06


def in_one_piece(arrays, axis, dim, along):
    ends, at = ([], 0)
    for a in arrays[:-1]:
        at += a.shape[along]
        ends.append(at)
    both = jnp.concatenate(arrays, axis=along)
    return tuple(jnp.split(lax.all_gather(both, axis, axis=dim, tiled=True), ends, axis=along))


def rms_scaled(values_in):
    return values_in * lax.rsqrt(jnp.mean(values_in * values_in, axis=-1, keepdims=True) + epsilon)


def expert_partial(row_block, gate_matrix, up_matrix, down_matrix):
    gate_part = jnp.dot(row_block, gate_matrix, preferred_element_type=jnp.float32)
    up_part = jnp.dot(row_block, up_matrix, preferred_element_type=jnp.float32)
    hidden = (jax.nn.silu(gate_part) * up_part).astype(jnp.bfloat16)
    return jnp.dot(hidden, down_matrix, preferred_element_type=jnp.float32)


def choice_ranks(routes, experts_all):
    flat_routes = routes.reshape(routes.shape[:-2] + (-1,))
    onehot = (flat_routes[..., None] == jnp.arange(experts_all, dtype=jnp.int32)).astype(jnp.int32)
    before = jnp.cumsum(onehot, axis=-2) - onehot
    return jnp.sum(before * onehot, axis=-1).reshape(routes.shape)


def slot_tokens(slot_index, targets, missing):
    flat_slots = slot_index.reshape(-1)
    owners = jnp.arange(flat_slots.shape[0], dtype=jnp.int32) // 2
    matches = flat_slots[None, :] == jnp.arange(targets, dtype=jnp.int32)[:, None]
    owner_found = jnp.sum(jnp.where(matches, owners[None, :], 0), axis=1)
    return jnp.where(jnp.any(matches, axis=1), owner_found, missing)


def on_device(
    queries,
    keys,
    values,
    key_bias,
    head_gain,
    out_weight,
    residual,
    norm_gain,
    gate_proj,
    up_proj,
    down_proj,
    expert_choice,
    expert_weights,
):
    rows_own = queries.shape[0]
    heads_here = head_gain.shape[0]
    head_size = head_gain.shape[1]
    model_width = out_weight.shape[1]
    seq_devices = lax.axis_size("sp")
    head_devices = lax.axis_size("tp")
    own_start = lax.axis_index("sp") * rows_own
    query_pos = own_start + jnp.arange(rows_own, dtype=jnp.int32)
    query_heads = queries.reshape(rows_own, heads_here, head_size)

    def key_block(slot_state, key_rows, value_rows, bias_rows, key_start):
        key_heads = key_rows.reshape(rows_own, heads_here, head_size)
        value_heads = value_rows.reshape(rows_own, heads_here, head_size)
        scores = jnp.einsum(
            "qhd,khd->hqk", query_heads, key_heads, preferred_element_type=jnp.float32
        ) * head_size ** (-0.5)
        scores = scores + bias_rows.astype(jnp.float32).T[:, None, :]
        key_pos = key_start + jnp.arange(rows_own, dtype=jnp.int32)
        earlier = (key_pos[None, :] < query_pos[:, None])[None, :, :]
        log_drops = jnp.where(earlier, jax.nn.log_sigmoid(-scores), 0.0)
        suffix = lax.cumsum(log_drops, axis=2, reverse=True) - log_drops
        within = jnp.where(earlier, jnp.exp(jax.nn.log_sigmoid(scores) + suffix), 0.0).astype(
            jnp.bfloat16
        )
        block_part = jnp.einsum(
            "hqk,khd->qhd", within, value_heads, preferred_element_type=jnp.float32
        )
        block_index = key_start // rows_own
        sums_new = lax.dynamic_update_index_in_dim(
            slot_state[0], block_part.reshape(rows_own, heads_here * head_size), block_index, 0
        )
        totals_new = lax.dynamic_update_index_in_dim(
            slot_state[1], jnp.sum(log_drops, axis=2), block_index, 0
        )
        return (sums_new, totals_new)

    empty_state = (
        jnp.zeros((seq_devices, rows_own, heads_here * head_size), jnp.float32),
        jnp.zeros((seq_devices, heads_here, rows_own), jnp.float32),
    )
    key_piece, value_piece, bias_piece = in_one_piece((keys, values, key_bias), "sp", 0, 1)

    def visit(block_count, state_in):
        offset = block_count * rows_own

        def take_rows(array):
            return lax.dynamic_slice_in_dim(array, offset, rows_own, 0)

        def compute(state_now):
            return key_block(
                state_now,
                take_rows(key_piece),
                take_rows(value_piece),
                take_rows(bias_piece),
                offset,
            )

        def keep(state_now):
            return state_now

        return lax.cond(offset <= own_start, compute, keep, state_in)

    block_sums, totals = lax.fori_loop(0, key_piece.shape[0] // rows_own, visit, empty_state)
    carried = jnp.sum(totals, axis=0, keepdims=True) - jnp.cumsum(totals, axis=0)
    factors = jnp.exp(carried).transpose(0, 2, 1)[..., None]
    mixture = jnp.sum(
        factors * block_sums.reshape(seq_devices, rows_own, heads_here, head_size), axis=0
    )
    attended = (
        (rms_scaled(mixture) * head_gain)
        .astype(jnp.bfloat16)
        .reshape(rows_own, heads_here * head_size)
    )
    row_share = rows_own // head_devices
    merged = lax.all_to_all(attended, "tp", split_axis=0, concat_axis=1, tiled=True)
    projected = jnp.dot(
        merged,
        lax.all_gather(out_weight, "tp", axis=0, tiled=True),
        preferred_element_type=jnp.float32,
    )
    stream = (residual.astype(jnp.float32) + projected).astype(jnp.bfloat16)
    normed = (rms_scaled(stream.astype(jnp.float32)) * norm_gain).astype(jnp.bfloat16)
    local_experts = gate_proj.shape[0]
    experts_all = local_experts * seq_devices
    capacity = 4 * rows_own // (head_devices * experts_all)
    own_slots = expert_choice * capacity + choice_ranks(expert_choice, experts_all)
    wanted = slot_tokens(own_slots, experts_all * capacity, row_share)
    outgoing = jnp.take(normed, wanted, axis=0, mode="fill", fill_value=0)
    arrived = lax.all_to_all(
        outgoing.reshape(seq_devices, local_experts, capacity, model_width),
        "sp",
        split_axis=0,
        concat_axis=0,
        tiled=True,
    )
    row_piece = lax.all_gather(arrived, "tp", axis=0, tiled=True)
    count_rows = row_piece.shape[0]
    partials = jnp.stack(
        [
            expert_partial(
                row_piece[:, 0].reshape(-1, model_width), gate_proj[0], up_proj[0], down_proj[0]
            ).reshape(count_rows, capacity, model_width)
        ],
        axis=1,
    )
    summed = lax.psum_scatter(partials.astype(jnp.bfloat16), "tp", scatter_dimension=0, tiled=True)
    returned = lax.all_to_all(summed, "sp", split_axis=0, concat_axis=0, tiled=True).reshape(
        experts_all * capacity, model_width
    )
    picked = jnp.take(returned, own_slots, axis=0).astype(jnp.float32)
    combined = jnp.sum(expert_weights[:, :, None] * picked, axis=1)
    return (stream.astype(jnp.float32) + combined).astype(jnp.bfloat16)


def solution(mesh):
    placed = (
        P("sp", "tp"),
        P("sp", "tp"),
        P("sp", "tp"),
        P("sp", "tp"),
        P("tp", None),
        P("tp", None),
        P(("sp", "tp"), None),
        P(),
        P("sp", None, "tp"),
        P("sp", None, "tp"),
        P("sp", "tp", None),
        P(("sp", "tp"), None),
        P(("sp", "tp"), None),
    )
    return jax.shard_map(
        on_device, mesh=mesh, in_specs=placed, out_specs=P(("sp", "tp"), None), check_vma=False
    )
```

profile of v0, /device:TPU:24, one launch (start us, length us, event | category | flops | bytes accessed | tf_op | source)
XLA Modules:
  0.0 623.0 jit_solution(17657157115760941867)
XLA Ops:
  15.2 54.8 %all-gather.4.cloned.1.call-done = bf16[6144,258]{0,1:T(8,128)(2,1)} async-done(((bf16[384,258]{0,1:T(8,128)(2,1)}), bf16[6144,258]{0,1:T(8,128)(2,1)}) %all-gather.4.cloned.1.call-update) | async-done | bytes 3170320 | tf_op jit(solution)/shard_map/all_gather | solution.py:15
  78.1 265.5 %while.17 = (s32[]{:T(128)}, f32[16,384,128]{1,2,0:T(8,128)}, f32[16,2,384]{2,1,0:T(2,128)}, s32[]{:T(128)}, bf16[6144,128]{0,1:T(8,128)(2,1)}, /*index=5*/bf16[...) while((s32[]{:T(128)}, f32[16,384,128]{1,2,0:T(8,128)}, ...), condition=%wide.region_6.7_spmd.clone.clone, body=%wide.region_0.6_spmd.clone.clone.sunk | while | flops 122542848 | bytes 19914736 | solution.py:121
  78.1 20.5 %conditional.4 = ((f32[16,384,128]{1,2,0:T(8,128)}, f32[16,2,384]{2,1,0:T(2,128)})) conditional(s32[]{:T(128)} %convert_element_type.76, (f32[16,384,128]{1,2,0:T(8,128)}, f32[16,2,384]{2,1,0:T(2,128)}) %tuple.55, (s32[]{:T(128)}, bf16[6144,128]{0,1:T(8,128)(2,1)}, s32[]{:T(128)}, bf16[6144,128]{0,1:T(8,128)(2,1)}, bf16[384,2,64]{0,2,1:T(8,128)(2,1)}, ...), branch_computations={%region_1.0_spmd, %region_2.5_spmd} | conditional | flops 122542848 | bytes 19912984 | solution.py:119
  98.6 20.4 %conditional.4 = ((f32[16,384,128]{1,2,0:T(8,128)}, f32[16,2,384]{2,1,0:T(2,128)})) conditional(s32[]{:T(128)} %convert_element_type.76, (f32[16,384,128]{1,2,0:T(8,128)}, f32[16,2,384]{2,1,0:T(2,128)}) %tuple.55, (s32[]{:T(128)}, bf16[6144,128]{0,1:T(8,128)(2,1)}, s32[]{:T(128)}, bf16[6144,128]{0,1:T(8,128)(2,1)}, bf16[384,2,64]{0,2,1:T(8,128)(2,1)}, ...), branch_computations={%region_1.0_spmd, %region_2.5_spmd} | conditional | flops 122542848 | bytes 19912984 | solution.py:119
  119.0 20.3 %conditional.4 = ((f32[16,384,128]{1,2,0:T(8,128)}, f32[16,2,384]{2,1,0:T(2,128)})) conditional(s32[]{:T(128)} %convert_element_type.76, (f32[16,384,128]{1,2,0:T(8,128)}, f32[16,2,384]{2,1,0:T(2,128)}) %tuple.55, (s32[]{:T(128)}, bf16[6144,128]{0,1:T(8,128)(2,1)}, s32[]{:T(128)}, bf16[6144,128]{0,1:T(8,128)(2,1)}, bf16[384,2,64]{0,2,1:T(8,128)(2,1)}, ...), branch_computations={%region_1.0_spmd, %region_2.5_spmd} | conditional | flops 122542848 | bytes 19912984 | solution.py:119
  139.4 20.4 %conditional.4 = ((f32[16,384,128]{1,2,0:T(8,128)}, f32[16,2,384]{2,1,0:T(2,128)})) conditional(s32[]{:T(128)} %convert_element_type.76, (f32[16,384,128]{1,2,0:T(8,128)}, f32[16,2,384]{2,1,0:T(2,128)}) %tuple.55, (s32[]{:T(128)}, bf16[6144,128]{0,1:T(8,128)(2,1)}, s32[]{:T(128)}, bf16[6144,128]{0,1:T(8,128)(2,1)}, bf16[384,2,64]{0,2,1:T(8,128)(2,1)}, ...), branch_computations={%region_1.0_spmd, %region_2.5_spmd} | conditional | flops 122542848 | bytes 19912984 | solution.py:119
  159.8 20.4 %conditional.4 = ((f32[16,384,128]{1,2,0:T(8,128)}, f32[16,2,384]{2,1,0:T(2,128)})) conditional(s32[]{:T(128)} %convert_element_type.76, (f32[16,384,128]{1,2,0:T(8,128)}, f32[16,2,384]{2,1,0:T(2,128)}) %tuple.55, (s32[]{:T(128)}, bf16[6144,128]{0,1:T(8,128)(2,1)}, s32[]{:T(128)}, bf16[6144,128]{0,1:T(8,128)(2,1)}, bf16[384,2,64]{0,2,1:T(8,128)(2,1)}, ...), branch_computations={%region_1.0_spmd, %region_2.5_spmd} | conditional | flops 122542848 | bytes 19912984 | solution.py:119
  180.2 20.4 %conditional.4 = ((f32[16,384,128]{1,2,0:T(8,128)}, f32[16,2,384]{2,1,0:T(2,128)})) conditional(s32[]{:T(128)} %convert_element_type.76, (f32[16,384,128]{1,2,0:T(8,128)}, f32[16,2,384]{2,1,0:T(2,128)}) %tuple.55, (s32[]{:T(128)}, bf16[6144,128]{0,1:T(8,128)(2,1)}, s32[]{:T(128)}, bf16[6144,128]{0,1:T(8,128)(2,1)}, bf16[384,2,64]{0,2,1:T(8,128)(2,1)}, ...), branch_computations={%region_1.0_spmd, %region_2.5_spmd} | conditional | flops 122542848 | bytes 19912984 | solution.py:119
  200.6 20.4 %conditional.4 = ((f32[16,384,128]{1,2,0:T(8,128)}, f32[16,2,384]{2,1,0:T(2,128)})) conditional(s32[]{:T(128)} %convert_element_type.76, (f32[16,384,128]{1,2,0:T(8,128)}, f32[16,2,384]{2,1,0:T(2,128)}) %tuple.55, (s32[]{:T(128)}, bf16[6144,128]{0,1:T(8,128)(2,1)}, s32[]{:T(128)}, bf16[6144,128]{0,1:T(8,128)(2,1)}, bf16[384,2,64]{0,2,1:T(8,128)(2,1)}, ...), branch_computations={%region_1.0_spmd, %region_2.5_spmd} | conditional | flops 122542848 | bytes 19912984 | solution.py:119
  221.0 20.4 %conditional.4 = ((f32[16,384,128]{1,2,0:T(8,128)}, f32[16,2,384]{2,1,0:T(2,128)})) conditional(s32[]{:T(128)} %convert_element_type.76, (f32[16,384,128]{1,2,0:T(8,128)}, f32[16,2,384]{2,1,0:T(2,128)}) %tuple.55, (s32[]{:T(128)}, bf16[6144,128]{0,1:T(8,128)(2,1)}, s32[]{:T(128)}, bf16[6144,128]{0,1:T(8,128)(2,1)}, bf16[384,2,64]{0,2,1:T(8,128)(2,1)}, ...), branch_computations={%region_1.0_spmd, %region_2.5_spmd} | conditional | flops 122542848 | bytes 19912984 | solution.py:119
  241.4 20.4 %conditional.4 = ((f32[16,384,128]{1,2,0:T(8,128)}, f32[16,2,384]{2,1,0:T(2,128)})) conditional(s32[]{:T(128)} %convert_element_type.76, (f32[16,384,128]{1,2,0:T(8,128)}, f32[16,2,384]{2,1,0:T(2,128)}) %tuple.55, (s32[]{:T(128)}, bf16[6144,128]{0,1:T(8,128)(2,1)}, s32[]{:T(128)}, bf16[6144,128]{0,1:T(8,128)(2,1)}, bf16[384,2,64]{0,2,1:T(8,128)(2,1)}, ...), branch_computations={%region_1.0_spmd, %region_2.5_spmd} | conditional | flops 122542848 | bytes 19912984 | solution.py:119
  261.8 20.4 %conditional.4 = ((f32[16,384,128]{1,2,0:T(8,128)}, f32[16,2,384]{2,1,0:T(2,128)})) conditional(s32[]{:T(128)} %convert_element_type.76, (f32[16,384,128]{1,2,0:T(8,128)}, f32[16,2,384]{2,1,0:T(2,128)}) %tuple.55, (s32[]{:T(128)}, bf16[6144,128]{0,1:T(8,128)(2,1)}, s32[]{:T(128)}, bf16[6144,128]{0,1:T(8,128)(2,1)}, bf16[384,2,64]{0,2,1:T(8,128)(2,1)}, ...), branch_computations={%region_1.0_spmd, %region_2.5_spmd} | conditional | flops 122542848 | bytes 19912984 | solution.py:119
  282.2 20.4 %conditional.4 = ((f32[16,384,128]{1,2,0:T(8,128)}, f32[16,2,384]{2,1,0:T(2,128)})) conditional(s32[]{:T(128)} %convert_element_type.76, (f32[16,384,128]{1,2,0:T(8,128)}, f32[16,2,384]{2,1,0:T(2,128)}) %tuple.55, (s32[]{:T(128)}, bf16[6144,128]{0,1:T(8,128)(2,1)}, s32[]{:T(128)}, bf16[6144,128]{0,1:T(8,128)(2,1)}, bf16[384,2,64]{0,2,1:T(8,128)(2,1)}, ...), branch_computations={%region_1.0_spmd, %region_2.5_spmd} | conditional | flops 122542848 | bytes 19912984 | solution.py:119
  302.6 20.4 %conditional.4 = ((f32[16,384,128]{1,2,0:T(8,128)}, f32[16,2,384]{2,1,0:T(2,128)})) conditional(s32[]{:T(128)} %convert_element_type.76, (f32[16,384,128]{1,2,0:T(8,128)}, f32[16,2,384]{2,1,0:T(2,128)}) %tuple.55, (s32[]{:T(128)}, bf16[6144,128]{0,1:T(8,128)(2,1)}, s32[]{:T(128)}, bf16[6144,128]{0,1:T(8,128)(2,1)}, bf16[384,2,64]{0,2,1:T(8,128)(2,1)}, ...), branch_computations={%region_1.0_spmd, %region_2.5_spmd} | conditional | flops 122542848 | bytes 19912984 | solution.py:119
  323.0 20.4 %conditional.4 = ((f32[16,384,128]{1,2,0:T(8,128)}, f32[16,2,384]{2,1,0:T(2,128)})) conditional(s32[]{:T(128)} %convert_element_type.76, (f32[16,384,128]{1,2,0:T(8,128)}, f32[16,2,384]{2,1,0:T(2,128)}) %tuple.55, (s32[]{:T(128)}, bf16[6144,128]{0,1:T(8,128)(2,1)}, s32[]{:T(128)}, bf16[6144,128]{0,1:T(8,128)(2,1)}, bf16[384,2,64]{0,2,1:T(8,128)(2,1)}, ...), branch_computations={%region_1.0_spmd, %region_2.5_spmd} | conditional | flops 122542848 | bytes 19912984 | solution.py:119
  356.4 8.2 %all-to-all-done = bf16[16,24,128]{2,1,0:T(8,128)(2,1)S(1)} async-done(((bf16[16,24,128]{2,1,0:T(8,128)(2,1)}), bf16[16,24,128]{2,1,0:T(8,128)(2,1)S(1)}, u32[]{:S(2)}, u32[]{:S(2)}) %all-to-all-start) | async-done | bytes 98336 | tf_op jit(solution)/shard_map/all_to_all | solution.py:133
  371.4 75.5 %all_to_all.26 = bf16[16,1,6,2048]{3,2,1,0:T(8,128)(2,1)S(1)} all-to-all(bf16[16,1,6,2048]{3,2,1,0:T(8,128)(2,1)S(1)} %select_bitcast_fusion), channel_id=1, replica_groups=mesh['sp'=16,'tp'=16] {'sp'}, dimensions={0} | all-to-all | bytes 786432 | tf_op jit(solution)/shard_map/all_to_all | solution.py:147
  447.8 40.8 %all-gather.8.cloned.1.call-done = bf16[256,1,6,2048]{3,0,2,1:T(8,128)(2,1)} async-done(((bf16[16,1,6,2048]{3,0,2,1:T(8,128)(2,1)}), bf16[256,1,6,2048]{3,0,2,1:T(8,128)(2,1)}) %all-gather.8.cloned.1.call-update) | async-done | bytes 6291472 | tf_op jit(solution)/shard_map/all_gather | solution.py:154
  488.7 9.6 %copy.109 = bf16[256,1,6,2048]{3,2,0,1:T(8,128)(2,1)} copy(bf16[256,1,6,2048]{3,0,2,1:T(8,128)(2,1)} %all-gather.8.cloned.1.call-done) | data formatting | bytes 12582912 | tf_op jit(solution)/shard_map/all_gather | solution.py:154
  498.3 11.1 %reshape_squeeze.3 = bf16[1536,2048]{1,0:T(8,128)(2,1)} reshape(bf16[256,1,6,2048]{3,2,0,1:T(8,128)(2,1)} %copy.109) | data formatting | bytes 12582912 | tf_op jit(solution)/shard_map/reshape;squeeze | solution.py:159
  523.0 7.5 %convert_bitcast_fusion.1 = bf16[256,1,6,2048]{3,0,2,1:T(8,128)(2,1)} fusion(bf16[1,448,2048]{2,1,0:T(8,128)(2,1)S(1)} %copy-done, bf16[256,6,448]{2,1,0:T(8,128)(2,1)} %dot_general.23), kind=kOutput, calls=%fused_computation.29 | convolution fusion | flops 2821718016 | bytes 9502720 | tf_op jit(solution)/shard_map/dot_general | solution.py:26
  530.5 65.8 %reduce-scatter.2.cloned.1.call-done = bf16[16,1,6,2048]{3,0,2,1:T(8,128)(2,1)} async-done(((bf16[256,1,6,2048]{3,0,2,1:T(8,128)(2,1)}), bf16[16,1,6,2048]{3,0,2,1:T(8,128)(2,1)}) %reduce-scatter.2.cloned.1.call-update) | async-done | bytes 393232 | tf_op jit(solution)/shard_map/reduce_scatter | solution.py:164
  598.3 7.2 %all-to-all-start.2 = ((bf16[16,1,6,2048]{3,2,1,0:T(8,128)(2,1)}), bf16[16,1,6,2048]{3,2,1,0:T(8,128)(2,1)S(1)}, u32[]{:S(2)}, u32[]{:S(2)}) async-start(bf16[16,1,6,2048]{3,2,1,0:T(8,128)(2,1)} %copy.112), calls=%async_computation.3 | async-start | bytes 1048576 | tf_op jit(solution)/shard_map/all_to_all | solution.py:165
  606.0 7.4 %all-to-all-done.2 = bf16[16,1,6,2048]{3,2,1,0:T(8,128)(2,1)S(1)} async-done(((bf16[16,1,6,2048]{3,2,1,0:T(8,128)(2,1)}), bf16[16,1,6,2048]{3,2,1,0:T(8,128)(2,1)S(1)}, u32[]{:S(2)}, u32[]{:S(2)}) %all-to-all-start.2) | async-done | bytes 393248 | tf_op jit(solution)/shard_map/all_to_all | solution.py:165
  (393 shorter events, 320.3 us)
Async XLA Ops:
  6.5 516.4 %copy-start = (bf16[1,448,2048]{2,1,0:T(8,128)(2,1)S(1)}, bf16[1,448,2048]{2,1,0:T(8,128)(2,1)}, u32[]{:S(2)}) copy-start(bf16[1,448,2048]{2,1,0:T(8,128)(2,1)} %param.27) | copy-start | bytes 5505028
  6.5 4.4 copy-start.7
  6.5 5.1 copy-start.18
  6.5 5.7 copy-start.13
  6.5 63.4 %all-gather.4.cloned.1.call-start = ((), (), s32[]{:S(2)}) async-start(), calls=%async_computation.4 | async-start | bytes 3446784 | tf_op jit(solution)/shard_map/all_gather | solution.py:15
  10.1 354.5 %all-gather.6.cloned.1.call-start = ((), (), s32[]{:S(2)}) async-start(), calls=%async_computation.5 | async-start | bytes 8912896 | tf_op jit(solution)/shard_map/all_gather | solution.py:136
  13.5 61.9 %copy-start.10 = (s32[24,2]{0,1:T(2,128)}, s32[24,2]{0,1:T(2,128)S(1)}, u32[]{:S(2)}) copy-start(s32[24,2]{0,1:T(2,128)S(1)} %get-tuple-element.261) | copy-start | bytes 580
  94.1 2.9 copy-start.2
  114.6 2.8 copy-start.2
  216.6 2.8 copy-start.2
  277.8 2.8 copy-start.2
  347.5 8.9 %copy-start.9 = (s32[16,6]{1,0:T(8,128)S(1)}, s32[16,6]{1,0:T(8,128)}, u32[]{:S(2)}) copy-start(s32[16,6]{1,0:T(8,128)} %select_n.105) | copy-start | bytes 1156
  347.5 17.2 %copy-start.6 = (bf16[24,2048]{1,0:T(8,128)(2,1)S(1)}, bf16[24,2048]{1,0:T(8,128)(2,1)}, u32[]{:S(2)}) copy-start(bf16[24,2048]{1,0:T(8,128)(2,1)} %param.23) | copy-start | bytes 294916
  349.2 15.4 %all-to-all-start = ((bf16[16,24,128]{2,1,0:T(8,128)(2,1)}), bf16[16,24,128]{2,1,0:T(8,128)(2,1)S(1)}, u32[]{:S(2)}, u32[]{:S(2)}) async-start(bf16[16,24,128]{2,1,0:T(8,128)(2,1)} %multiply_convert_fusion.1), calls=%async_computation | async-start | bytes 196608 | tf_op jit(solution)/shard_map/all_to_all | solution.py:133
  356.3 132.3 %all-gather.8.cloned.1.call-start = ((), (), s32[]{:S(2)}) async-start(), calls=%async_computation.6 | async-start | bytes 6684672 | tf_op jit(solution)/shard_map/all_gather | solution.py:154
  356.4 13.6 %copy-start.12 = (f32[2048]{0:T(1024)S(1)}, f32[2048]{0:T(1024)}, u32[]{:S(2)}) copy-start(f32[2048]{0:T(1024)} %param.24) | copy-start | bytes 24580
  447.8 148.5 %reduce-scatter.2.cloned.1.call-start = ((), (), s32[]{:S(2)}) async-start(), calls=%async_computation.7 | async-start | bytes 6684672 | tf_op jit(solution)/shard_map/reduce_scatter | solution.py:164
  509.3 5.9 copy-start.3
  509.3 5.9 copy-start.17
  530.5 75.1 %copy-start.11 = (s32[24,2]{0,1:T(2,128)S(1)}, s32[24,2]{0,1:T(2,128)}, u32[]{:S(2)}) copy-start(s32[24,2]{0,1:T(2,128)} %copy-done.10) | copy-start | bytes 580
  530.5 75.3 %copy-start.14 = (pred[24,2]{0,1:T(4,128)(4,1)S(1)}, pred[24,2]{0,1:T(4,128)(4,1)}, u32[]{:S(2)}) copy-start(pred[24,2]{0,1:T(4,128)(4,1)} %get-tuple-element.260) | copy-start | bytes 148
  530.5 75.4 %copy-start.15 = (f32[24,2]{0,1:T(2,128)S(1)}, f32[24,2]{0,1:T(2,128)}, u32[]{:S(2)}) copy-start(f32[24,2]{0,1:T(2,128)} %param.29) | copy-start | bytes 580
  598.3 15.1 %all-to-all-start.2 = ((bf16[16,1,6,2048]{3,2,1,0:T(8,128)(2,1)}), bf16[16,1,6,2048]{3,2,1,0:T(8,128)(2,1)S(1)}, u32[]{:S(2)}, u32[]{:S(2)}) async-start(bf16[16,1,6,2048]{3,2,1,0:T(8,128)(2,1)} %copy.112), calls=%async_computation.3 | async-start | bytes 1048576 | tf_op jit(solution)/shard_map/all_to_all | solution.py:165
  606.0 9.8 %copy-start.5 = (f32[24,2048]{1,0:T(8,128)S(1)}, f32[24,2048]{1,0:T(8,128)}, u32[]{:S(2)}) copy-start(f32[24,2048]{1,0:T(8,128)} %copy-done.4) | copy-start | bytes 589828
  (37 other events, 77.9 us)
Sparse Core Ops, SparseCore 0:
  10.3 59.6 all-gather.3
  71.8 55.6 all-gather.5
  447.9 40.6 all-gather.7
  530.6 65.6 reduce-scatter.1
where the time goes:
time: 629 us; the launch traced here: 623 us
  waiting for transfers between devices  178 us (28%)
  other arithmetic  154 us (24%)
  local copies, waits for them, and re-layouts  115 us (18%)
  blocking collectives  75.5 us (12%)
  matrix products  71.9 us (11%)
  starting transfers between devices  14.5 us (2%)
  between operations  13.5 us (2%)
    another operation x26, other arithmetic  108 us
    all_to_all x1, blocking collectives, on_device(): lax.all_to_all(outgoing.reshape(seq_devices, local_experts, capacity, mod...  75.5 us
    reduce_scatter x1, waiting for transfers between devices, on_device(): lax.psum_scatter(partials.astype(jnp.bfloat16), 'tp', scatter_dimension=0...  65.8 us
    all_gather x1, waiting for transfers between devices, in_one_piece(): lax.all_gather(both, axis, axis=dim, tiled=True)  54.8 us
    dot_general x13, matrix products, key_block(): jnp.einsum('qhd,khd->hqk', query_heads, key_heads, preferred_element_type...  46.7 us
    all_gather x1, waiting for transfers between devices, on_device(): row_piece = lax.all_gather(arrived, 'tp', axis=0, tiled=True)  40.8 us
    convert_element_type x13, other arithmetic, key_block(): jnp.where(earlier, jnp.exp(jax.nn.log_sigmoid(scores) + suffix), 0.0)  21.4 us
    dynamic_slice x13, local copies, waits for them, and re-layouts, take_rows(): return lax.dynamic_slice_in_dim(array, offset, rows_own, 0)  20.7 us
  transfers between devices with their start and end apart: 6, of which 5 were waited for; matrix products, arithmetic and copies ran while one was open for 43% of the time, Pallas kernels for 0%

commit v1 on v0

--- a/solution.py
+++ b/solution.py
@@ -1,9 +1,14 @@
+import functools
+
 import jax
 import jax.numpy as jnp
 from jax import lax
+from jax.experimental import pallas as pl
+from jax.experimental.pallas import tpu as pltpu
 from jax.sharding import PartitionSpec as P
 
 epsilon = 1e-06
+CHUNK = 256
 
 
 def in_one_piece(arrays, axis, dim, along):
@@ -17,6 +22,81 @@
 
 def rms_scaled(values_in):
     return values_in * lax.rsqrt(jnp.mean(values_in * values_in, axis=-1, keepdims=True) + epsilon)
+
+
+def attention_kernel(heads, head_size, q_ref, k_ref, v_ref, b_ref, gain_ref, out_ref, acc, carry):
+    rows = q_ref.shape[0]
+    own = lax.axis_index("sp")
+    acc[...] = jnp.zeros_like(acc)
+    carry[...] = jnp.zeros_like(carry)
+    row = lax.broadcasted_iota(jnp.int32, (CHUNK, CHUNK), 0)
+    col = lax.broadcasted_iota(jnp.int32, (CHUNK, CHUNK), 1)
+    after = (row > col).astype(jnp.bfloat16)
+
+    def chunk(start, masked, query_offset):
+        for h in range(heads):
+            lanes = slice(h * head_size, (h + 1) * head_size)
+            q_neg = q_ref[:, lanes] * jnp.bfloat16(-(head_size ** -0.5))
+            k_part = k_ref[pl.ds(start, CHUNK), lanes]
+            minus = lax.dot_general(
+                q_neg, k_part, (((1,), (1,)), ((), ())), preferred_element_type=jnp.float32
+            ) - b_ref[pl.ds(h, 1), pl.ds(start, CHUNK)]
+            log_part = jnp.log(1.0 + jnp.exp(-jnp.abs(minus)))
+            drop = jnp.minimum(minus, 0.0) - log_part
+            own_log = drop - minus
+            if masked:
+                q_at = lax.broadcasted_iota(jnp.int32, (rows, CHUNK), 0) + query_offset
+                k_at = lax.broadcasted_iota(jnp.int32, (rows, CHUNK), 1)
+                earlier = k_at < q_at
+                drop = jnp.where(earlier, drop, 0.0)
+            suffix = jnp.dot(drop.astype(jnp.bfloat16), after, preferred_element_type=jnp.float32)
+            within = jnp.exp(own_log + suffix)
+            if masked:
+                within = jnp.where(earlier, within, 0.0)
+            part = jnp.dot(
+                within.astype(jnp.bfloat16), v_ref[pl.ds(start, CHUNK), lanes], preferred_element_type=jnp.float32
+            )
+            now = carry[h]
+            acc[h] += jnp.exp(now) * part
+            carry[h] = now + (suffix[:, :1] + drop[:, :1])
+
+    def pair(index, masked):
+        base = pl.multiple_of((own - 2 * index) * rows, 128)
+        for c in reversed(range(2 * rows // CHUNK)):
+            chunk(base + c * CHUNK, masked, rows - c * CHUNK)
+
+    pair(0, True)
+
+    def body(index, none):
+        pair(index, False)
+        return none
+
+    lax.fori_loop(1, (own + 2) // 2, body, 0)
+    for h in range(heads):
+        mixture = acc[h]
+        scaled = mixture * lax.rsqrt(jnp.mean(mixture * mixture, axis=-1, keepdims=True) + epsilon)
+        out_ref[:, h * head_size : (h + 1) * head_size] = (scaled * gain_ref[pl.ds(h, 1), :]).astype(jnp.bfloat16)
+
+
+def attention(queries, keys, values, bias, gain):
+    rows = queries.shape[0]
+    heads, head_size = gain.shape
+    keys = jnp.pad(keys, ((rows, 0), (0, 0)))
+    values = jnp.pad(values, ((rows, 0), (0, 0)))
+    bias = jnp.pad(bias.astype(jnp.float32).T, ((0, 0), (rows, 0)), constant_values=-30000.0)
+    vmem = pl.BlockSpec(memory_space=pltpu.VMEM)
+    return pl.pallas_call(
+        functools.partial(attention_kernel, heads, head_size),
+        out_shape=jax.ShapeDtypeStruct(queries.shape, jnp.bfloat16),
+        in_specs=[vmem] * 5,
+        out_specs=vmem,
+        scratch_shapes=[
+            pltpu.VMEM((heads, rows, head_size), jnp.float32),
+            pltpu.VMEM((heads, rows, 1), jnp.float32),
+        ],
+        compiler_params=pltpu.CompilerParams(vmem_limit_bytes=32 << 20),
+        name="attention",
+    )(queries, keys, values, bias, gain)
 
 
 def expert_partial(row_block, gate_matrix, up_matrix, down_matrix):
@@ -57,78 +137,11 @@
     expert_weights,
 ):
     rows_own = queries.shape[0]
-    heads_here = head_gain.shape[0]
-    head_size = head_gain.shape[1]
     model_width = out_weight.shape[1]
     seq_devices = lax.axis_size("sp")
     head_devices = lax.axis_size("tp")
-    own_start = lax.axis_index("sp") * rows_own
-    query_pos = own_start + jnp.arange(rows_own, dtype=jnp.int32)
-    query_heads = queries.reshape(rows_own, heads_here, head_size)
-
-    def key_block(slot_state, key_rows, value_rows, bias_rows, key_start):
-        key_heads = key_rows.reshape(rows_own, heads_here, head_size)
-        value_heads = value_rows.reshape(rows_own, heads_here, head_size)
-        scores = jnp.einsum(
-            "qhd,khd->hqk", query_heads, key_heads, preferred_element_type=jnp.float32
-        ) * head_size ** (-0.5)
-        scores = scores + bias_rows.astype(jnp.float32).T[:, None, :]
-        key_pos = key_start + jnp.arange(rows_own, dtype=jnp.int32)
-        earlier = (key_pos[None, :] < query_pos[:, None])[None, :, :]
-        log_drops = jnp.where(earlier, jax.nn.log_sigmoid(-scores), 0.0)
-        suffix = lax.cumsum(log_drops, axis=2, reverse=True) - log_drops
-        within = jnp.where(earlier, jnp.exp(jax.nn.log_sigmoid(scores) + suffix), 0.0).astype(
-            jnp.bfloat16
-        )
-        block_part = jnp.einsum(
-            "hqk,khd->qhd", within, value_heads, preferred_element_type=jnp.float32
-        )
-        block_index = key_start // rows_own
-        sums_new = lax.dynamic_update_index_in_dim(
-            slot_state[0], block_part.reshape(rows_own, heads_here * head_size), block_index, 0
-        )
-        totals_new = lax.dynamic_update_index_in_dim(
-            slot_state[1], jnp.sum(log_drops, axis=2), block_index, 0
-        )
-        return (sums_new, totals_new)
-
-    empty_state = (
-        jnp.zeros((seq_devices, rows_own, heads_here * head_size), jnp.float32),
-        jnp.zeros((seq_devices, heads_here, rows_own), jnp.float32),
-    )
     key_piece, value_piece, bias_piece = in_one_piece((keys, values, key_bias), "sp", 0, 1)
-
-    def visit(block_count, state_in):
-        offset = block_count * rows_own
-
-        def take_rows(array):
-            return lax.dynamic_slice_in_dim(array, offset, rows_own, 0)
-
-        def compute(state_now):
-            return key_block(
-                state_now,
-                take_rows(key_piece),
-                take_rows(value_piece),
-                take_rows(bias_piece),
-                offset,
-            )
-
-        def keep(state_now):
-            return state_now
-
-        return lax.cond(offset <= own_start, compute, keep, state_in)
-
-    block_sums, totals = lax.fori_loop(0, key_piece.shape[0] // rows_own, visit, empty_state)
-    carried = jnp.sum(totals, axis=0, keepdims=True) - jnp.cumsum(totals, axis=0)
-    factors = jnp.exp(carried).transpose(0, 2, 1)[..., None]
-    mixture = jnp.sum(
-        factors * block_sums.reshape(seq_devices, rows_own, heads_here, head_size), axis=0
-    )
-    attended = (
-        (rms_scaled(mixture) * head_gain)
-        .astype(jnp.bfloat16)
-        .reshape(rows_own, heads_here * head_size)
-    )
+    attended = attention(queries, key_piece, value_piece, bias_piece, head_gain)
     row_share = rows_own // head_devices
     merged = lax.all_to_all(attended, "tp", split_axis=0, concat_axis=1, tiled=True)
     projected = jnp.dot(

time: 629 us -> 333 us (0.53)
  other arithmetic: 154 us -> 5.84 us
  local copies, waits for them, and re-layouts: 115 us -> 43.4 us
  blocking collectives: 75.5 us -> 16.7 us
  matrix products: 71.9 us -> 22.4 us
  waiting for transfers between devices: 178 us -> 199 us
  Pallas kernels: 0 us -> 15.9 us
    another operation x40 -> x0, other arithmetic: 113 us -> none
    all_to_all x1, blocking collectives: 75.5 us -> 16.7 us  [on_device(): lax.all_to_all(outgoing.reshape(seq_devices, local_experts, capacity, mod...]
    dot_general x26 -> x0, matrix products: 49.5 us -> none  [the longest x13 46.7 us: key_block(): jnp.einsum('qhd,khd->hqk', query_heads, key_heads, preferred_element_type...]
    convert_element_type x14 -> x0, other arithmetic: 22.1 us -> none  [the longest x13 21.4 us: key_block(): jnp.where(earlier, jnp.exp(jax.nn.log_sigmoid(scores) + suffix), 0.0)]
    dynamic_slice x13 -> x0, local copies, waits for them, and re-layouts: 20.7 us -> none  [take_rows(): return lax.dynamic_slice_in_dim(array, offset, rows_own, 0)]
    another operation x39 -> x0, local copies, waits for them, and re-layouts: 18.1 us -> none
    dynamic_update_slice x26 -> x0, local copies, waits for them, and re-layouts: 16.8 us -> none  [the longest x13 9.16 us: key_block(): lax.dynamic_update_index_in_dim(slot_state[0], block_part.reshape(rows_ow...]
    all_gather x1, waiting for transfers between devices: 0.01 us -> 16 us  [on_device(): lax.all_gather(out_weight, 'tp', axis=0, tiled=True)]
  transfers between devices with their start and end apart: 6 -> 6, of which waited for: 5 -> 6; matrix products, arithmetic and copies ran while one was open for 43% -> 4% of each run, Pallas kernels for 0% -> 5%
where the time goes in v1:
time: 333 us; the launch traced here: 331 us
  waiting for transfers between devices  199 us (60%)
  local copies, waits for them, and re-layouts  43.4 us (13%)
  matrix products  22.4 us (7%)
  blocking collectives  16.7 us (5%)
  Pallas kernels  15.9 us (5%)
  starting transfers between devices  14.6 us (4%)
  between operations  13.4 us (4%)
  other arithmetic  5.84 us (2%)
    reduce_scatter x1, waiting for transfers between devices, on_device(): lax.psum_scatter(partials.astype(jnp.bfloat16), 'tp', scatter_dimension=0...  65.9 us
    all_gather x1, waiting for transfers between devices, in_one_piece(): lax.all_gather(both, axis, axis=dim, tiled=True)  56.5 us
    all_gather x1, waiting for transfers between devices, on_device(): row_piece = lax.all_gather(arrived, 'tp', axis=0, tiled=True)  42.7 us
    all_to_all x1, blocking collectives, on_device(): lax.all_to_all(outgoing.reshape(seq_devices, local_experts, capacity, mod...  16.7 us
    all_gather x1, waiting for transfers between devices, on_device(): lax.all_gather(out_weight, 'tp', axis=0, tiled=True)  16 us
    pallas_call x1, Pallas kernels, attention(): pl.pallas_call(functools.partial(attention_kernel, heads, head_size), out...  15.9 us
    another operation x1, local copies, waits for them, and re-layouts, on_device(): row_piece[:, 0].reshape(-1, model_width)  11 us
    all_gather x1, local copies, waits for them, and re-layouts, on_device(): row_piece = lax.all_gather(arrived, 'tp', axis=0, tiled=True)  9.61 us
  transfers between devices with their start and end apart: 6, of which 6 were waited for; matrix products, arithmetic and copies ran while one was open for 4% of the time, Pallas kernels for 5%

profile of v1, /device:TPU:24, one launch (start us, length us, event | category | flops | bytes accessed | tf_op | source)
XLA Modules:
  0.0 330.9 jit_solution(11549045927359267088)
XLA Ops:
  8.7 1.4 pad_maximum_fusion
  13.4 56.5 %all-gather.4.cloned.1.call-done = bf16[6144,258]{0,1:T(8,128)(2,1)} async-done(((bf16[384,258]{0,1:T(8,128)(2,1)}), bf16[6144,258]{0,1:T(8,128)(2,1)}) %all-gather.4.cloned.1.call-update) | async-done | bytes 3170320 | tf_op jit(solution)/shard_map/all_gather | solution.py:20
  69.9 3.9 %fusion.13 = (bf16[6144,128]{0,1:T(8,128)(2,1)}, bf16[6144,128]{0,1:T(8,128)(2,1)}) fusion(bf16[6144,258]{0,1:T(8,128)(2,1)} %all-gather.4.cloned.1.call-done), kind=kLoop, calls=%fused_computation.44 | loop fusion | bytes 6291456 | tf_op jit(solution)/shard_map/split | solution.py:20
  73.8 1.9 copy.82
  75.8 2.6 copy.83
  80.9 15.9 %attention.1 = bf16[384,128]{1,0:T(8,128)(2,1)} custom-call(bf16[384,128]{1,0:T(8,128)(2,1)S(1)} %copy-done.1, bf16[6528,128]{1,0:T(8,128)(2,1)S(1)} %pad.11.clone.k_ref, bf16[6528,128]{1,0:T(8,128)(2,1)S(1)} %pad.12.clone.v_ref, f32[2,6528]{1,0:T(2,128)S(1)} %pad.13.b_ref, f32[2,64]{1,0:T(2,128)S(1)} %copy-done.2), custom_call_target="tpu_custom_call" | custom-call | tf_op jit(solution)/shard_map/attention/pallas_call | solution.py:88
  96.7 7.1 %all-to-all-start = ((bf16[16,24,128]{2,1,0:T(8,128)(2,1)}), bf16[16,24,128]{2,1,0:T(8,128)(2,1)S(1)}, u32[]{:S(2)}, u32[]{:S(2)}) async-start(bf16[16,24,128]{2,1,0:T(8,128)(2,1)} %bitcast.1), calls=%async_computation | async-start | bytes 196608 | tf_op jit(solution)/shard_map/all_to_all | solution.py:146
  103.9 9.6 %all-to-all-done = bf16[16,24,128]{2,1,0:T(8,128)(2,1)S(1)} async-done(((bf16[16,24,128]{2,1,0:T(8,128)(2,1)}), bf16[16,24,128]{2,1,0:T(8,128)(2,1)S(1)}, u32[]{:S(2)}, u32[]{:S(2)}) %all-to-all-start) | async-done | bytes 98336 | tf_op jit(solution)/shard_map/all_to_all | solution.py:146
  113.5 16.0 %all-gather.6.cloned.1.call-done = bf16[2048,2048]{1,0:T(8,128)(2,1)} async-done(((bf16[128,2048]{1,0:T(8,128)(2,1)}), bf16[2048,2048]{1,0:T(8,128)(2,1)}) %all-gather.6.cloned.1.call-update) | async-done | bytes 8388624 | tf_op jit(solution)/shard_map/all_gather | solution.py:149
  129.5 4.7 %multiply_reduce_fusion.1 = (f32[24]{0:T(128)S(1)}, f32[24,2048]{1,0:T(8,128)S(1)}) fusion(bf16[2048,2048]{1,0:T(8,128)(2,1)} %all-gather.6.cloned.1.call-done, bf16[24,2048]{1,0:T(8,128)(2,1)S(1)} %copy-done.7, bf16[16,24,128]{2,1,0:T(8,128)(2,1)S(1)} %all-to-all-done), kind=kOutput, calls=%fused_computation.19 | convolution fusion | flops 201621472 | bytes 8781920 | tf_op jit(solution)/shard_map/dot_general | solution.py:147
  136.1 16.7 %all_to_all.29 = bf16[16,1,6,2048]{3,2,1,0:T(8,128)(2,1)S(1)} all-to-all(bf16[16,1,6,2048]{3,2,1,0:T(8,128)(2,1)S(1)} %select_bitcast_fusion), channel_id=1, replica_groups=mesh['sp'=16,'tp'=16] {'sp'}, dimensions={0} | all-to-all | bytes 786432 | tf_op jit(solution)/shard_map/all_to_all | solution.py:160
  154.0 42.7 %all-gather.8.cloned.1.call-done = bf16[256,1,6,2048]{3,0,2,1:T(8,128)(2,1)} async-done(((bf16[16,1,6,2048]{3,0,2,1:T(8,128)(2,1)}), bf16[256,1,6,2048]{3,0,2,1:T(8,128)(2,1)}) %all-gather.8.cloned.1.call-update) | async-done | bytes 6291472 | tf_op jit(solution)/shard_map/all_gather | solution.py:167
  196.6 9.6 %copy.77 = bf16[256,1,6,2048]{3,2,0,1:T(8,128)(2,1)} copy(bf16[256,1,6,2048]{3,0,2,1:T(8,128)(2,1)} %all-gather.8.cloned.1.call-done) | data formatting | bytes 12582912 | tf_op jit(solution)/shard_map/all_gather | solution.py:167
  206.2 11.0 %reshape_squeeze.3 = bf16[1536,2048]{1,0:T(8,128)(2,1)} reshape(bf16[256,1,6,2048]{3,2,0,1:T(8,128)(2,1)} %copy.77) | data formatting | bytes 12582912 | tf_op jit(solution)/shard_map/reshape;squeeze | solution.py:172
  217.3 5.9 %fusion.5 = f32[1536,448]{0,1:T(8,128)S(1)} fusion(bf16[1536,2048]{1,0:T(8,128)(2,1)} %reshape_squeeze.3, bf16[1,2048,448]{1,2,0:T(8,128)(2,1)} %param.21), kind=kOutput, calls=%fused_computation.10 | convolution fusion | flops 2818572288 | bytes 10878976 | tf_op jit(solution)/shard_map/dot_general | solution.py:103
  223.2 4.3 %fusion = bf16[1536,448]{0,1:T(8,128)(2,1)} fusion(bf16[1536,2048]{1,0:T(8,128)(2,1)S(1)} %copy-done.3, f32[1536,448]{0,1:T(8,128)S(1)} %fusion.5, bf16[1,2048,448]{1,2,0:T(8,128)(2,1)S(1)} %copy-done.10), kind=kOutput, calls=%fused_computation.4 | convolution fusion | flops 2822701056 | bytes 12255232 | tf_op jit(solution)/shard_map/dot_general | solution.py:104
  227.5 1.7 copy.78
  229.2 1.7 dot_general.17
  230.9 7.5 %convert_bitcast_fusion = bf16[256,1,6,2048]{3,0,2,1:T(8,128)(2,1)} fusion(bf16[1,448,2048]{2,1,0:T(8,128)(2,1)S(1)} %copy-done, bf16[256,6,448]{2,1,0:T(8,128)(2,1)} %dot_general.17), kind=kOutput, calls=%fused_computation.2 | convolution fusion | flops 2821718016 | bytes 9502720 | tf_op jit(solution)/shard_map/dot_general | solution.py:106
  238.4 65.9 %reduce-scatter.2.cloned.1.call-done = bf16[16,1,6,2048]{3,0,2,1:T(8,128)(2,1)} async-done(((bf16[256,1,6,2048]{3,0,2,1:T(8,128)(2,1)}), bf16[16,1,6,2048]{3,0,2,1:T(8,128)(2,1)}) %reduce-scatter.2.cloned.1.call-update) | async-done | bytes 393232 | tf_op jit(solution)/shard_map/reduce_scatter | solution.py:177
  304.3 2.0 copy.80
  306.3 7.2 %all-to-all-start.2 = ((bf16[16,1,6,2048]{3,2,1,0:T(8,128)(2,1)}), bf16[16,1,6,2048]{3,2,1,0:T(8,128)(2,1)S(1)}, u32[]{:S(2)}, u32[]{:S(2)}) async-start(bf16[16,1,6,2048]{3,2,1,0:T(8,128)(2,1)} %copy.80), calls=%async_computation.3 | async-start | bytes 1048576 | tf_op jit(solution)/shard_map/all_to_all | solution.py:178
  313.9 7.5 %all-to-all-done.2 = bf16[16,1,6,2048]{3,2,1,0:T(8,128)(2,1)S(1)} async-done(((bf16[16,1,6,2048]{3,2,1,0:T(8,128)(2,1)}), bf16[16,1,6,2048]{3,2,1,0:T(8,128)(2,1)S(1)}, u32[]{:S(2)}, u32[]{:S(2)}) %all-to-all-start.2) | async-done | bytes 393248 | tf_op jit(solution)/shard_map/all_to_all | solution.py:178
  322.3 1.4 multiply_reduce_fusion
  (69 shorter events, 13.1 us)
Async XLA Ops:
  6.5 224.3 %copy-start = (bf16[1,448,2048]{2,1,0:T(8,128)(2,1)S(1)}, bf16[1,448,2048]{2,1,0:T(8,128)(2,1)}, u32[]{:S(2)}) copy-start(bf16[1,448,2048]{2,1,0:T(8,128)(2,1)} %param.23) | copy-start | bytes 5505028
  6.5 63.4 %all-gather.4.cloned.1.call-start = ((), (), s32[]{:S(2)}) async-start(), calls=%async_computation.4 | async-start | bytes 3446784 | tf_op jit(solution)/shard_map/all_gather | solution.py:20
  10.1 119.4 %all-gather.6.cloned.1.call-start = ((), (), s32[]{:S(2)}) async-start(), calls=%async_computation.5 | async-start | bytes 8912896 | tf_op jit(solution)/shard_map/all_gather | solution.py:149
  78.3 1.4 copy-start.4
  78.3 2.5 copy-start.1
  78.3 2.5 copy-start.2
  79.9 49.6 %copy-start.7 = (bf16[24,2048]{1,0:T(8,128)(2,1)S(1)}, bf16[24,2048]{1,0:T(8,128)(2,1)}, u32[]{:S(2)}) copy-start(bf16[24,2048]{1,0:T(8,128)(2,1)} %param.19) | copy-start | bytes 294916
  96.7 16.8 %all-to-all-start = ((bf16[16,24,128]{2,1,0:T(8,128)(2,1)}), bf16[16,24,128]{2,1,0:T(8,128)(2,1)S(1)}, u32[]{:S(2)}, u32[]{:S(2)}) async-start(bf16[16,24,128]{2,1,0:T(8,128)(2,1)} %bitcast.1), calls=%async_computation | async-start | bytes 196608 | tf_op jit(solution)/shard_map/all_to_all | solution.py:146
  103.8 92.8 %all-gather.8.cloned.1.call-start = ((), (), s32[]{:S(2)}) async-start(), calls=%async_computation.6 | async-start | bytes 6684672 | tf_op jit(solution)/shard_map/all_gather | solution.py:167
  103.9 31.0 %copy-start.8 = (f32[2048]{0:T(1024)S(1)}, f32[2048]{0:T(1024)}, u32[]{:S(2)}) copy-start(f32[2048]{0:T(1024)} %param.20) | copy-start | bytes 24580
  134.2 0.7 copy-start.5
  153.7 150.5 %reduce-scatter.2.cloned.1.call-start = ((), (), s32[]{:S(2)}) async-start(), calls=%async_computation.7 | async-start | bytes 6684672 | tf_op jit(solution)/shard_map/reduce_scatter | solution.py:177
  217.3 5.9 %copy-start.3 = (bf16[1536,2048]{1,0:T(8,128)(2,1)S(1)}, bf16[1536,2048]{1,0:T(8,128)(2,1)}, u32[]{:S(2)}) copy-start(bf16[1536,2048]{1,0:T(8,128)(2,1)} %reshape_squeeze.3) | copy-start | bytes 18874372
  217.3 5.9 %copy-start.10 = (bf16[1,2048,448]{1,2,0:T(8,128)(2,1)S(1)}, bf16[1,2048,448]{1,2,0:T(8,128)(2,1)}, u32[]{:S(2)}) copy-start(bf16[1,2048,448]{1,2,0:T(8,128)(2,1)} %param.22) | copy-start | bytes 5505028
  238.4 75.4 %copy-start.9 = (f32[24,2]{0,1:T(2,128)S(1)}, f32[24,2]{0,1:T(2,128)}, u32[]{:S(2)}) copy-start(f32[24,2]{0,1:T(2,128)} %param.25) | copy-start | bytes 580
  238.4 85.3 %copy-start.6 = (f32[24,2048]{1,0:T(8,128)S(1)}, f32[24,2048]{1,0:T(8,128)}, u32[]{:S(2)}) copy-start(f32[24,2048]{1,0:T(8,128)} %copy-done.5) | copy-start | bytes 589828
  306.3 15.1 %all-to-all-start.2 = ((bf16[16,1,6,2048]{3,2,1,0:T(8,128)(2,1)}), bf16[16,1,6,2048]{3,2,1,0:T(8,128)(2,1)S(1)}, u32[]{:S(2)}, u32[]{:S(2)}) async-start(bf16[16,1,6,2048]{3,2,1,0:T(8,128)(2,1)} %copy.80), calls=%async_computation.3 | async-start | bytes 1048576 | tf_op jit(solution)/shard_map/all_to_all | solution.py:178
Sparse Core Ops, SparseCore 0:
  10.2 59.6 all-gather.3
  71.7 57.7 all-gather.5
  153.9 42.7 all-gather.7
  238.5 65.7 reduce-scatter.1

commit v2 on v1

--- a/solution.py
+++ b/solution.py
@@ -99,13 +99,6 @@
     )(queries, keys, values, bias, gain)
 
 
-def expert_partial(row_block, gate_matrix, up_matrix, down_matrix):
-    gate_part = jnp.dot(row_block, gate_matrix, preferred_element_type=jnp.float32)
-    up_part = jnp.dot(row_block, up_matrix, preferred_element_type=jnp.float32)
-    hidden = (jax.nn.silu(gate_part) * up_part).astype(jnp.bfloat16)
-    return jnp.dot(hidden, down_matrix, preferred_element_type=jnp.float32)
-
-
 def choice_ranks(routes, experts_all):
     flat_routes = routes.reshape(routes.shape[:-2] + (-1,))
     onehot = (flat_routes[..., None] == jnp.arange(experts_all, dtype=jnp.int32)).astype(jnp.int32)
@@ -113,12 +106,385 @@
     return jnp.sum(before * onehot, axis=-1).reshape(routes.shape)
 
 
-def slot_tokens(slot_index, targets, missing):
-    flat_slots = slot_index.reshape(-1)
-    owners = jnp.arange(flat_slots.shape[0], dtype=jnp.int32) // 2
-    matches = flat_slots[None, :] == jnp.arange(targets, dtype=jnp.int32)[:, None]
-    owner_found = jnp.sum(jnp.where(matches, owners[None, :], 0), axis=1)
-    return jnp.where(jnp.any(matches, axis=1), owner_found, missing)
+MESH = pl.DeviceIdType.MESH
+SLOT_ROWS = 8
+
+
+def remote(src, dst, send_sem, recv_sem, device):
+    return pltpu.make_async_remote_copy(
+        src_ref=src, dst_ref=dst, send_sem=send_sem, recv_sem=recv_sem, device_id=device, device_id_type=MESH
+    )
+
+
+def expert_kernel(
+    cap, stream_ref, normed_ref, select_ref, weight_ref, gate_hbm, up_hbm, down_hbm, out_ref,
+    outgoing, arrived, rows, part, partner_part, ring_sum, back, returned, gate_w, up_w, down_w,
+    load_sem, go_send, go_recv, ag_send, ag_recv, pair_send, pair_recv, pin_send, pin_recv,
+    rs_send, rs_recv, back_send, back_recv,
+):
+    experts, _, width = outgoing.shape
+    chunks, chips, _, block, _ = rows.shape
+    far, half, per = chips // 2, width // 2, experts // chunks
+    me, t = lax.axis_index("sp"), lax.axis_index("tp")
+    z, c = t // 2, t % 2
+    partner = (me, 2 * z + (1 - c))
+    ahead = ((me, 2 * ((z + 1) % chips) + c), (me, 2 * ((z + chips - 1) % chips) + c))
+    piece = (pl.ds(0, half), pl.ds(half, half))
+
+    barrier = pltpu.get_barrier_semaphore()
+    for device in (partner, *ahead):
+        pl.semaphore_signal(barrier, inc=1, device_id=device, device_id_type=MESH)
+
+    def greet(j, none):
+        pl.semaphore_signal(barrier, inc=1, device_id=((me + j) % experts, t), device_id_type=MESH)
+        return none
+
+    lax.fori_loop(1, experts, greet, 0)
+    loads = [
+        pltpu.make_async_copy(src.at[0], dst, load_sem.at[i])
+        for i, (src, dst) in enumerate(((gate_hbm, gate_w), (up_hbm, up_w), (down_hbm, down_w)))
+    ]
+    for load in loads:
+        load.start()
+    chosen = jnp.dot(select_ref[...], normed_ref[...], preferred_element_type=jnp.float32)
+    outgoing[...] = chosen.reshape(experts, SLOT_ROWS, width).astype(jnp.bfloat16)
+    for k in range(chunks):
+        for d in range(2):
+            ring_sum[k, d, 0, :, piece[1 - d]] = jnp.zeros((block, half), jnp.bfloat16)
+    pl.semaphore_wait(barrier, experts + 2)
+
+    def go(src, dst, source_id, device):
+        return remote(src, dst, go_send.at[source_id], go_recv.at[source_id], device)
+
+    def send_go(j, none):
+        e = (me + j) % experts
+        remote(outgoing.at[e], arrived.at[me], go_send.at[e], go_recv.at[me], (e, t)).start()
+        return none
+
+    lax.fori_loop(1, experts, send_go, 0)
+    own = pltpu.make_async_copy(outgoing.at[me], arrived.at[me], go_recv.at[me])
+    own.start()
+
+    def take_arrived(k):
+        def wait_one(j, none):
+            s = k * per + j
+
+            @pl.when(s == me)
+            def _():
+                own.wait()
+
+            @pl.when(s != me)
+            def _():
+                remote(outgoing.at[s], arrived.at[s], go_send.at[s], go_recv.at[s], (s, t)).wait_recv()
+
+            return none
+
+        lax.fori_loop(0, per, wait_one, 0)
+        row = lax.broadcasted_iota(jnp.int32, (block, per * SLOT_ROWS), 0)
+        col = lax.broadcasted_iota(jnp.int32, (block, per * SLOT_ROWS), 1)
+        pick = (col == row // cap * SLOT_ROWS + row % cap).astype(jnp.bfloat16)
+        padded = arrived[pl.ds(k * per, per)].astype(jnp.float32).reshape(per * SLOT_ROWS, width)
+        rows[k, z, c] = jnp.dot(
+            pick, padded.astype(jnp.bfloat16), preferred_element_type=jnp.float32
+        ).astype(jnp.bfloat16)
+
+    def ring_rows(k, d, i, p, device):
+        at = (z - i if d == 0 else z + i) % chips if isinstance(i, int) else lax.rem((z - i if d == 0 else z + i) + chips, chips)
+        ref = rows.at[k, at, c, :, piece[p]]
+        return remote(ref, ref, ag_send.at[k, d, i, p], ag_recv.at[k, d, i, p], device)
+
+    def to_partner(k, at, p):
+        ref = rows.at[k, at, c, :, piece[p]]
+        return remote(ref, ref, pair_send.at[k, at, p], pair_recv.at[k, at, p], partner)
+
+    def start_own(k):
+        for p in range(2):
+            for d in range(2):
+                ring_rows(k, d, 0, p if d == 0 else 1 - p, ahead[d]).start()
+        for p in range(2):
+            to_partner(k, z, p).start()
+
+    def from_ring(k, d, i, p):
+        at = lax.rem((z - i - 1 if d == 0 else z + i + 1) + chips, chips)
+        ref = rows.at[k, at, c, :, piece[p]]
+        return at, remote(ref, ref, ag_send.at[k, d, i, p], ag_recv.at[k, d, i, p], ahead[d])
+
+    def gather_step(k, i):
+        for order in range(2):
+            for d in range(2):
+                p = d if order == 0 else 1 - d
+
+                def handle(d=d, p=p, last=(order == 1)):
+                    at, copy = from_ring(k, d, i, p)
+                    copy.wait_recv()
+
+                    @pl.when(i + 1 < (far - 1 if last else far))
+                    def _():
+                        ref = rows.at[k, at, c, :, piece[p]]
+                        remote(ref, ref, ag_send.at[k, d, i + 1, p], ag_recv.at[k, d, i + 1, p], ahead[d]).start()
+
+                    to_partner(k, at, p).start()
+
+                if order == 0:
+                    handle()
+                else:
+                    pl.when(i < far - 1)(handle)
+
+    def wait_partner_rows(k):
+        def wait_one(at, none):
+            for p in range(2):
+                ref = rows.at[k, at, 1 - c, :, piece[p]]
+                remote(ref, ref, pair_send.at[k, at, p], pair_recv.at[k, at, p], partner).wait_recv()
+            return none
+
+        lax.fori_loop(0, chips, wait_one, 0)
+
+    group = chips // far
+
+    def experts_on(k, i):
+        at = pl.ds(i * group, group)
+        x = rows[k, at].reshape(group * 2 * block, width)
+        gate = jnp.dot(x, gate_w[...], preferred_element_type=jnp.float32)
+        up = jnp.dot(x, up_w[...], preferred_element_type=jnp.float32)
+        hidden = (gate / (1.0 + jnp.exp(-gate)) * up).astype(jnp.bfloat16)
+        product = jnp.dot(hidden, down_w[...], preferred_element_type=jnp.float32)
+        part[k, at] = product.astype(jnp.bfloat16).reshape(group, 2, block, width)
+        for j in range(group):
+            pin(k, i * group + j).start()
+
+    def pin(k, at):
+        return remote(
+            part.at[k, at, 1 - c], partner_part.at[k, at], pin_send.at[k, at], pin_recv.at[k, at], partner
+        )
+
+    def wait_pins(k):
+        def wait_one(at, none):
+            pin(k, at).wait_recv()
+            return none
+
+        lax.fori_loop(0, chips, wait_one, 0)
+
+    def ring_step(k, i):
+        for order in range(2):
+            for d in range(2):
+                p = d if order == 0 else 1 - d
+
+                def handle(d=d, p=p, first=(order == 0)):
+                    at = lax.rem((z + (far - i) if d == 0 else z - (far - i)) + chips, chips)
+                    own_sum = part[k, at, c, :, piece[p]].astype(jnp.float32) + partner_part[
+                        k, at, :, piece[p]
+                    ].astype(jnp.float32)
+
+                    @pl.when(i == 0)
+                    def _():
+                        part[k, at, c, :, piece[p]] = own_sum.astype(jnp.bfloat16)
+
+                    @pl.when(i > 0)
+                    def _():
+                        before = jnp.maximum(i - 1, 0)
+                        if first:
+                            from_sum(k, d, before, p).wait_recv()
+                        else:
+                            pl.when(i > 1)(lambda: from_sum(k, d, before, p).wait_recv())
+                        total = own_sum + ring_sum[k, d, before, :, piece[p]].astype(jnp.float32)
+                        part[k, at, c, :, piece[p]] = total.astype(jnp.bfloat16)
+
+                    remote(
+                        part.at[k, at, c, :, piece[p]],
+                        ring_sum.at[k, d, i, :, piece[p]],
+                        rs_send.at[k, d, i, p],
+                        rs_recv.at[k, d, i, p],
+                        ahead[d],
+                    ).start()
+
+                if order == 0:
+                    handle()
+                else:
+                    pl.when(i > 0)(handle)
+
+    def from_sum(k, d, i, p):
+        ref = ring_sum.at[k, d, i, :, piece[p]]
+        return remote(ref, ref, rs_send.at[k, d, i, p], rs_recv.at[k, d, i, p], ahead[d])
+
+    def send_back(k):
+        for p in range(2):
+            for d in range(2):
+                from_sum(k, d, far - 1, p).wait_recv()
+        total = (
+            part[k, z, c].astype(jnp.float32)
+            + partner_part[k, z].astype(jnp.float32)
+            + ring_sum[k, 0, far - 1].astype(jnp.float32)
+            + ring_sum[k, 1, far - 1].astype(jnp.float32)
+        ).astype(jnp.bfloat16)
+        row = lax.broadcasted_iota(jnp.int32, (per * SLOT_ROWS, block), 0)
+        col = lax.broadcasted_iota(jnp.int32, (per * SLOT_ROWS, block), 1)
+        spread = ((row % SLOT_ROWS < cap) & (col == row // SLOT_ROWS * cap + row % SLOT_ROWS)).astype(jnp.bfloat16)
+        back[pl.ds(k * per, per)] = (
+            jnp.dot(spread, total, preferred_element_type=jnp.float32)
+            .reshape(per, SLOT_ROWS, width)
+            .astype(jnp.bfloat16)
+        )
+
+        def send_one(j, none):
+            s = k * per + j
+
+            @pl.when(s != me)
+            def _():
+                remote(back.at[s], returned.at[me], back_send.at[s], back_recv.at[me], (s, t)).start()
+
+            @pl.when(s == me)
+            def _():
+                pltpu.make_async_copy(back.at[s], returned.at[me], back_recv.at[me]).start()
+
+            return none
+
+        lax.fori_loop(0, per, send_one, 0)
+
+    def steps(body):
+        def one(i, none):
+            body(i)
+            return none
+
+        lax.fori_loop(0, far, one, 0)
+
+    take_arrived(0)
+    start_own(0)
+    take_arrived(1)
+    steps(lambda i: gather_step(0, i))
+    start_own(1)
+    for load in loads:
+        load.wait()
+    wait_partner_rows(0)
+
+    def gather_and_compute(i):
+        gather_step(1, i)
+        experts_on(0, i)
+
+    steps(gather_and_compute)
+    wait_partner_rows(1)
+    wait_pins(0)
+
+    def sum_and_compute(i):
+        ring_step(0, i)
+        experts_on(1, i)
+
+    steps(sum_and_compute)
+    wait_pins(1)
+    steps(lambda i: (pl.when(i == 1)(lambda: send_back(0)), ring_step(1, i)))
+    send_back(1)
+
+    def wait_back(e, none):
+        @pl.when(e == me)
+        def _():
+            pltpu.make_async_copy(back.at[e], returned.at[e], back_recv.at[e]).wait()
+
+        @pl.when(e != me)
+        def _():
+            remote(back.at[e], returned.at[e], back_send.at[e], back_recv.at[e], (e, t)).wait_recv()
+
+        return none
+
+    lax.fori_loop(0, experts, wait_back, 0)
+    weights = weight_ref[...]
+    high = weights.astype(jnp.bfloat16)
+    rest = weights - high.astype(jnp.float32)
+    middle = rest.astype(jnp.bfloat16)
+    low = (rest - middle.astype(jnp.float32)).astype(jnp.bfloat16)
+    picked = returned[...].astype(jnp.float32).reshape(experts * SLOT_ROWS, width).astype(jnp.bfloat16)
+    combined = stream_ref[...].astype(jnp.float32)
+    for share in (low, middle, high):
+        combined = combined + jnp.dot(share, picked, preferred_element_type=jnp.float32)
+    out_ref[...] = combined.astype(jnp.bfloat16)
+
+    def drain_sp(j, none):
+        e = (me + j) % experts
+        remote(outgoing.at[e], arrived.at[me], go_send.at[e], go_recv.at[me], (e, t)).wait_send()
+        remote(back.at[e], returned.at[me], back_send.at[e], back_recv.at[me], (e, t)).wait_send()
+        return none
+
+    lax.fori_loop(1, experts, drain_sp, 0)
+
+    def drain_pair(at, none):
+        for k in range(chunks):
+            for p in range(2):
+                to_partner(k, at, p).wait_send()
+            pin(k, at).wait_send()
+        return none
+
+    lax.fori_loop(0, chips, drain_pair, 0)
+
+    def drain_ring(i, none):
+        for k in range(chunks):
+            for d in range(2):
+                for p in range(2):
+
+                    def sent(k=k, d=d, p=p):
+                        ref = rows.at[k, 0, c, :, piece[p]]
+                        remote(ref, ref, ag_send.at[k, d, i, p], ag_recv.at[k, d, i, p], ahead[d]).wait_send()
+
+                    def summed(k=k, d=d, p=p):
+                        ref = rows.at[k, 0, c, :, piece[p]]
+                        remote(ref, ref, rs_send.at[k, d, i, p], rs_recv.at[k, d, i, p], ahead[d]).wait_send()
+
+                    if p == d:
+                        sent()
+                        summed()
+                    else:
+                        pl.when(i < far - 1)(sent)
+                        pl.when(i > 0)(summed)
+        return none
+
+    lax.fori_loop(0, far, drain_ring, 0)
+
+
+def expert_layer(stream, normed, choice, choice_weights, gate_proj, up_proj, down_proj, seq_devices, head_devices, cap):
+    own_rows, width = stream.shape
+    hidden = gate_proj.shape[2]
+    experts, chips, chunks = seq_devices, head_devices // 2, 2
+    far, block = chips // 2, seq_devices // chunks * cap
+    slots = choice * SLOT_ROWS + choice_ranks(choice, experts)
+    targets = jnp.arange(experts * SLOT_ROWS, dtype=jnp.int32)
+    match = slots[:, :, None] == targets[None, None, :]
+    select = jnp.any(match, axis=1).T.astype(jnp.bfloat16)
+    weights = jnp.sum(jnp.where(match, choice_weights[:, :, None], 0.0), axis=1)
+    vmem, hbm = pl.BlockSpec(memory_space=pltpu.VMEM), pl.BlockSpec(memory_space=pl.ANY)
+    bf16, dma = jnp.bfloat16, pltpu.SemaphoreType.DMA
+    return pl.pallas_call(
+        functools.partial(expert_kernel, cap),
+        out_shape=jax.ShapeDtypeStruct(stream.shape, bf16),
+        in_specs=[vmem] * 4 + [hbm] * 3,
+        out_specs=vmem,
+        scratch_shapes=[
+            pltpu.VMEM((experts, SLOT_ROWS, width), bf16),
+            pltpu.VMEM((experts, SLOT_ROWS, width), bf16),
+            pltpu.VMEM((chunks, chips, 2, block, width), bf16),
+            pltpu.VMEM((chunks, chips, 2, block, width), bf16),
+            pltpu.VMEM((chunks, chips, block, width), bf16),
+            pltpu.VMEM((chunks, 2, far, block, width), bf16),
+            pltpu.VMEM((experts, SLOT_ROWS, width), bf16),
+            pltpu.VMEM((experts, SLOT_ROWS, width), bf16),
+            pltpu.VMEM((width, hidden), bf16),
+            pltpu.VMEM((width, hidden), bf16),
+            pltpu.VMEM((hidden, width), bf16),
+            dma((3,)),
+            dma((experts,)),
+            dma((experts,)),
+            dma((chunks, 2, far, 2)),
+            dma((chunks, 2, far, 2)),
+            dma((chunks, chips, 2)),
+            dma((chunks, chips, 2)),
+            dma((chunks, chips)),
+            dma((chunks, chips)),
+            dma((chunks, 2, far, 2)),
+            dma((chunks, 2, far, 2)),
+            dma((experts,)),
+            dma((experts,)),
+        ],
+        compiler_params=pltpu.CompilerParams(
+            collective_id=1, has_side_effects=True, vmem_limit_bytes=56 << 20
+        ),
+        name="experts",
+    )(stream, normed, select, weights, gate_proj, up_proj, down_proj)
 
 
 def on_device(
@@ -151,36 +517,10 @@
     )
     stream = (residual.astype(jnp.float32) + projected).astype(jnp.bfloat16)
     normed = (rms_scaled(stream.astype(jnp.float32)) * norm_gain).astype(jnp.bfloat16)
-    local_experts = gate_proj.shape[0]
-    experts_all = local_experts * seq_devices
-    capacity = 4 * rows_own // (head_devices * experts_all)
-    own_slots = expert_choice * capacity + choice_ranks(expert_choice, experts_all)
-    wanted = slot_tokens(own_slots, experts_all * capacity, row_share)
-    outgoing = jnp.take(normed, wanted, axis=0, mode="fill", fill_value=0)
-    arrived = lax.all_to_all(
-        outgoing.reshape(seq_devices, local_experts, capacity, model_width),
-        "sp",
-        split_axis=0,
-        concat_axis=0,
-        tiled=True,
+    cap = 4 * rows_own // (head_devices * seq_devices)
+    return expert_layer(
+        stream, normed, expert_choice, expert_weights, gate_proj, up_proj, down_proj, seq_devices, head_devices, cap
     )
-    row_piece = lax.all_gather(arrived, "tp", axis=0, tiled=True)
-    count_rows = row_piece.shape[0]
-    partials = jnp.stack(
-        [
-            expert_partial(
-                row_piece[:, 0].reshape(-1, model_width), gate_proj[0], up_proj[0], down_proj[0]
-            ).reshape(count_rows, capacity, model_width)
-        ],
-        axis=1,
-    )
-    summed = lax.psum_scatter(partials.astype(jnp.bfloat16), "tp", scatter_dimension=0, tiled=True)
-    returned = lax.all_to_all(summed, "sp", split_axis=0, concat_axis=0, tiled=True).reshape(
-        experts_all * capacity, model_width
-    )
-    picked = jnp.take(returned, own_slots, axis=0).astype(jnp.float32)
-    combined = jnp.sum(expert_weights[:, :, None] * picked, axis=1)
-    return (stream.astype(jnp.float32) + combined).astype(jnp.bfloat16)
 
 
 def solution(mesh):

time: 333 us -> 245 us (0.74)
  waiting for transfers between devices: 199 us -> 79.1 us
  Pallas kernels: 15.9 us -> 117 us
  local copies, waits for them, and re-layouts: 43.4 us -> 18.1 us
  matrix products: 22.4 us -> 4.69 us
  blocking collectives: 16.7 us -> 0 us
  starting transfers between devices: 14.6 us -> 7.17 us
    pallas_call x0 -> x1, Pallas kernels: none -> 101 us  [expert_layer(): pl.pallas_call(functools.partial(expert_kernel, cap), out_shape=jax.Shape...]
    reduce_scatter x1 -> x0, waiting for transfers between devices: 65.9 us -> none  [on_device(): lax.psum_scatter(partials.astype(jnp.bfloat16), 'tp', scatter_dimension=0...]
    all_gather x1 -> x0, waiting for transfers between devices: 42.7 us -> none  [on_device(): row_piece = lax.all_gather(arrived, 'tp', axis=0, tiled=True)]
    dot_general x3 -> x0, matrix products: 17.7 us -> none  [the longest x1 7.48 us: expert_partial(): return jnp.dot(hidden, down_matrix, preferred_element_type=jnp.float32)]
    all_to_all x1 -> x0, blocking collectives: 16.7 us -> none  [on_device(): lax.all_to_all(outgoing.reshape(seq_devices, local_experts, capacity, mod...]
    another operation x1 -> x0, local copies, waits for them, and re-layouts: 11 us -> none  [on_device(): row_piece[:, 0].reshape(-1, model_width)]
    all_gather x1 -> x0, local copies, waits for them, and re-layouts: 9.61 us -> none  [on_device(): row_piece = lax.all_gather(arrived, 'tp', axis=0, tiled=True)]
    all_to_all x1, waiting for transfers between devices: 9.58 us -> 1.86 us  [on_device(): lax.all_to_all(attended, 'tp', split_axis=0, concat_axis=1, tiled=True)]
  transfers between devices with their start and end apart: 6 -> 3, of which waited for: 6 -> 3; matrix products, arithmetic and copies ran while one was open for 4% -> 7% of each run, Pallas kernels for 5% -> 6%
where the time goes in v2:
time: 245 us
  Pallas kernels  117 us (48%)
  waiting for transfers between devices  79.1 us (32%)
  local copies, waits for them, and re-layouts  18.1 us (7%)
  between operations  13.6 us (6%)
  starting transfers between devices  7.17 us (3%)
  other arithmetic  4.79 us (2%)
  matrix products  4.69 us (2%)
    pallas_call x1, Pallas kernels, expert_layer(): pl.pallas_call(functools.partial(expert_kernel, cap), out_shape=jax.Shape...  101 us
    all_gather x1, waiting for transfers between devices, in_one_piece(): lax.all_gather(both, axis, axis=dim, tiled=True)  57 us
    all_gather x1, waiting for transfers between devices, on_device(): lax.all_gather(out_weight, 'tp', axis=0, tiled=True)  19.5 us
    pallas_call x1, Pallas kernels, attention(): pl.pallas_call(functools.partial(attention_kernel, heads, head_size), out...  15.8 us
    unnamed x22, local copies, waits for them, and re-layouts  13.5 us
    all_to_all x1, starting transfers between devices, on_device(): lax.all_to_all(attended, 'tp', split_axis=0, concat_axis=1, tiled=True)  7.12 us
  transfers between devices with their start and end apart: 3, of which 3 were waited for; matrix products, arithmetic and copies ran while one was open for 7% of the time, Pallas kernels for 6%

profile of v2, /device:TPU:24, one launch (start us, length us, event | category | flops | bytes accessed | tf_op | source)
XLA Modules:
  0.0 244.6 jit_solution(10917067504027690328)
XLA Ops:
  6.5 1.0 copy.58
  7.5 1.0 copy.59
  8.6 1.4 pad_maximum_fusion
  10.0 0.7 all-gather.5.cloned.1.call-update
  10.7 0.8 copy.63
  11.7 0.2 select_reduce_fusion.1
  12.1 0.7 multiply_add_fusion
  12.8 57.0 %all-gather.3.cloned.1.call-done = bf16[6144,258]{0,1:T(8,128)(2,1)} async-done(((bf16[384,258]{0,1:T(8,128)(2,1)}), bf16[6144,258]{0,1:T(8,128)(2,1)}) %all-gather.3.cloned.1.call-update) | async-done | bytes 3170320 | tf_op jit(solution)/shard_map/all_gather | solution.py:20
  69.8 3.4 %fusion.8 = (bf16[6144,128]{0,1:T(8,128)(2,1)}, bf16[6144,128]{0,1:T(8,128)(2,1)S(1)}) fusion(bf16[6144,258]{0,1:T(8,128)(2,1)} %all-gather.3.cloned.1.call-done), kind=kLoop, calls=%fused_computation.19 | loop fusion | bytes 6291456 | tf_op jit(solution)/shard_map/split | solution.py:20
  73.1 0.9 copy.68
  74.0 1.9 copy.69
  76.2 0.9 convert_bitcast_fusion
  77.2 15.8 %attention.1 = bf16[384,128]{1,0:T(8,128)(2,1)} custom-call(bf16[384,128]{1,0:T(8,128)(2,1)S(1)} %copy-done, bf16[6528,128]{1,0:T(8,128)(2,1)S(1)} %pad.11.clone.k_ref, bf16[6528,128]{1,0:T(8,128)(2,1)S(1)} %pad.12.clone.v_ref, f32[2,6528]{1,0:T(2,128)S(1)} %pad.13.b_ref, f32[2,64]{1,0:T(2,128)S(1)} %copy-done.1), custom_call_target="tpu_custom_call" | custom-call | tf_op jit(solution)/shard_map/attention/pallas_call | solution.py:88
  93.0 7.1 %all-to-all-start = ((bf16[16,24,128]{2,1,0:T(8,128)(2,1)}), bf16[16,24,128]{2,1,0:T(8,128)(2,1)S(1)}, u32[]{:S(2)}, u32[]{:S(2)}) async-start(bf16[16,24,128]{2,1,0:T(8,128)(2,1)} %bitcast.1), calls=%async_computation | async-start | bytes 196608 | tf_op jit(solution)/shard_map/all_to_all | solution.py:512
  100.2 0.7 copy.65
  101.0 2.4 copy.66.gate_hbm
  103.4 3.9 %copy.67.up_hbm = bf16[1,2048,448]{2,1,0:T(8,128)(2,1)} copy(bf16[1,2048,448]{1,2,0:T(8,128)(2,1)} %param.22) | data formatting | bytes 3670016 | tf_op args[9]
  107.3 0.7 select_reduce_fusion.weight_ref
  107.9 1.9 all-to-all-done
  109.8 19.5 %all-gather.5.cloned.1.call-done = bf16[2048,2048]{1,0:T(8,128)(2,1)} async-done(((bf16[128,2048]{1,0:T(8,128)(2,1)}), bf16[2048,2048]{1,0:T(8,128)(2,1)}) %all-gather.5.cloned.1.call-update) | async-done | bytes 8388624 | tf_op jit(solution)/shard_map/all_gather | solution.py:515
  129.4 4.7 %fusion.1 = (f32[24]{0:T(128)S(1)}, bf16[24,2048]{1,0:T(8,128)(2,1)S(1)}) fusion(bf16[2048,2048]{1,0:T(8,128)(2,1)} %all-gather.5.cloned.1.call-done, bf16[24,2048]{1,0:T(8,128)(2,1)S(1)} %copy-done.4, bf16[16,24,128]{2,1,0:T(8,128)(2,1)S(1)} %all-to-all-done), kind=kOutput, calls=%fused_computation.5 | convolution fusion | flops 201621472 | bytes 8683616 | tf_op jit(solution)/shard_map/dot_general | solution.py:513
  134.1 0.7 fusion.3.normed_ref
  134.8 101.4 %experts.1 = bf16[24,2048]{1,0:T(8,128)(2,1)} custom-call(bf16[24,2048]{1,0:T(8,128)(2,1)} %copy-done.3, bf16[24,2048]{1,0:T(8,128)(2,1)} %fusion.3.normed_ref, bf16[128,24]{1,0:T(8,128)(2,1)} %bitcast.15, f32[24,128]{1,0:T(8,128)} %select_reduce_fusion.weight_ref, bf16[1,2048,448]{2,1,0:T(8,128)(2,1)} %copy.66.gate_hbm, bf16[1,2048,448]{2,1,0:T(8,128)(2,1)} %copy.67.up_hbm, ...), custom_call_target="tpu_custom_call" | custom-call | tf_op jit(solution)/shard_map/experts/pallas_call | solution.py:452
  236.2 1.5 copy.78
  (28 shorter events, 0.9 us)
Async XLA Ops:
  6.5 63.2 %all-gather.3.cloned.1.call-start = ((), (), s32[]{:S(2)}) async-start(), calls=%async_computation.1 | async-start | bytes 3446784 | tf_op jit(solution)/shard_map/all_gather | solution.py:20
  10.0 119.4 %all-gather.5.cloned.1.call-start = ((), (), s32[]{:S(2)}) async-start(), calls=%async_computation.2 | async-start | bytes 8912896 | tf_op jit(solution)/shard_map/all_gather | solution.py:515
  76.1 1.1 copy-start
  76.1 1.1 copy-start.1
  77.2 23.8 %copy-start.2 = (bf16[1,2048,448]{1,2,0:T(8,128)(2,1)S(1)}, bf16[1,2048,448]{1,2,0:T(8,128)(2,1)}, u32[]{:S(2)}) copy-start(bf16[1,2048,448]{1,2,0:T(8,128)(2,1)} %param.21) | copy-start | bytes 5505028
  93.0 16.8 %all-to-all-start = ((bf16[16,24,128]{2,1,0:T(8,128)(2,1)}), bf16[16,24,128]{2,1,0:T(8,128)(2,1)S(1)}, u32[]{:S(2)}, u32[]{:S(2)}) async-start(bf16[16,24,128]{2,1,0:T(8,128)(2,1)} %bitcast.1), calls=%async_computation | async-start | bytes 196608 | tf_op jit(solution)/shard_map/all_to_all | solution.py:512
  103.4 3.9 %copy-start.6 = (f32[24,2]{0,1:T(2,128)S(1)}, f32[24,2]{0,1:T(2,128)}, u32[]{:S(2)}) copy-start(f32[24,2]{0,1:T(2,128)} %param.25) | copy-start | bytes 580
  103.4 26.0 %copy-start.4 = (bf16[24,2048]{1,0:T(8,128)(2,1)S(1)}, bf16[24,2048]{1,0:T(8,128)(2,1)}, u32[]{:S(2)}) copy-start(bf16[24,2048]{1,0:T(8,128)(2,1)} %param.19) | copy-start | bytes 294916
  107.9 26.1 %copy-start.5 = (f32[2048]{0:T(1024)S(1)}, f32[2048]{0:T(1024)}, u32[]{:S(2)}) copy-start(f32[2048]{0:T(1024)} %param.20) | copy-start | bytes 24580
  134.1 0.8 copy-start.3
Sparse Core Ops, SparseCore 0:
  10.1 59.6 all-gather.2
  71.6 57.7 all-gather.4

commit v3 on v2

--- a/solution.py
+++ b/solution.py
@@ -9,94 +9,14 @@
 
 epsilon = 1e-06
 CHUNK = 256
-
-
-def in_one_piece(arrays, axis, dim, along):
-    ends, at = ([], 0)
-    for a in arrays[:-1]:
-        at += a.shape[along]
-        ends.append(at)
-    both = jnp.concatenate(arrays, axis=along)
-    return tuple(jnp.split(lax.all_gather(both, axis, axis=dim, tiled=True), ends, axis=along))
-
-
-def rms_scaled(values_in):
-    return values_in * lax.rsqrt(jnp.mean(values_in * values_in, axis=-1, keepdims=True) + epsilon)
-
-
-def attention_kernel(heads, head_size, q_ref, k_ref, v_ref, b_ref, gain_ref, out_ref, acc, carry):
-    rows = q_ref.shape[0]
-    own = lax.axis_index("sp")
-    acc[...] = jnp.zeros_like(acc)
-    carry[...] = jnp.zeros_like(carry)
-    row = lax.broadcasted_iota(jnp.int32, (CHUNK, CHUNK), 0)
-    col = lax.broadcasted_iota(jnp.int32, (CHUNK, CHUNK), 1)
-    after = (row > col).astype(jnp.bfloat16)
-
-    def chunk(start, masked, query_offset):
-        for h in range(heads):
-            lanes = slice(h * head_size, (h + 1) * head_size)
-            q_neg = q_ref[:, lanes] * jnp.bfloat16(-(head_size ** -0.5))
-            k_part = k_ref[pl.ds(start, CHUNK), lanes]
-            minus = lax.dot_general(
-                q_neg, k_part, (((1,), (1,)), ((), ())), preferred_element_type=jnp.float32
-            ) - b_ref[pl.ds(h, 1), pl.ds(start, CHUNK)]
-            log_part = jnp.log(1.0 + jnp.exp(-jnp.abs(minus)))
-            drop = jnp.minimum(minus, 0.0) - log_part
-            own_log = drop - minus
-            if masked:
-                q_at = lax.broadcasted_iota(jnp.int32, (rows, CHUNK), 0) + query_offset
-                k_at = lax.broadcasted_iota(jnp.int32, (rows, CHUNK), 1)
-                earlier = k_at < q_at
-                drop = jnp.where(earlier, drop, 0.0)
-            suffix = jnp.dot(drop.astype(jnp.bfloat16), after, preferred_element_type=jnp.float32)
-            within = jnp.exp(own_log + suffix)
-            if masked:
-                within = jnp.where(earlier, within, 0.0)
-            part = jnp.dot(
-                within.astype(jnp.bfloat16), v_ref[pl.ds(start, CHUNK), lanes], preferred_element_type=jnp.float32
-            )
-            now = carry[h]
-            acc[h] += jnp.exp(now) * part
-            carry[h] = now + (suffix[:, :1] + drop[:, :1])
-
-    def pair(index, masked):
-        base = pl.multiple_of((own - 2 * index) * rows, 128)
-        for c in reversed(range(2 * rows // CHUNK)):
-            chunk(base + c * CHUNK, masked, rows - c * CHUNK)
-
-    pair(0, True)
-
-    def body(index, none):
-        pair(index, False)
-        return none
-
-    lax.fori_loop(1, (own + 2) // 2, body, 0)
-    for h in range(heads):
-        mixture = acc[h]
-        scaled = mixture * lax.rsqrt(jnp.mean(mixture * mixture, axis=-1, keepdims=True) + epsilon)
-        out_ref[:, h * head_size : (h + 1) * head_size] = (scaled * gain_ref[pl.ds(h, 1), :]).astype(jnp.bfloat16)
-
-
-def attention(queries, keys, values, bias, gain):
-    rows = queries.shape[0]
-    heads, head_size = gain.shape
-    keys = jnp.pad(keys, ((rows, 0), (0, 0)))
-    values = jnp.pad(values, ((rows, 0), (0, 0)))
-    bias = jnp.pad(bias.astype(jnp.float32).T, ((0, 0), (rows, 0)), constant_values=-30000.0)
-    vmem = pl.BlockSpec(memory_space=pltpu.VMEM)
-    return pl.pallas_call(
-        functools.partial(attention_kernel, heads, head_size),
-        out_shape=jax.ShapeDtypeStruct(queries.shape, jnp.bfloat16),
-        in_specs=[vmem] * 5,
-        out_specs=vmem,
-        scratch_shapes=[
-            pltpu.VMEM((heads, rows, head_size), jnp.float32),
-            pltpu.VMEM((heads, rows, 1), jnp.float32),
-        ],
-        compiler_params=pltpu.CompilerParams(vmem_limit_bytes=32 << 20),
-        name="attention",
-    )(queries, keys, values, bias, gain)
+MESH = pl.DeviceIdType.MESH
+SLOT_ROWS = 8
+
+
+def remote(src, dst, send_sem, recv_sem, device):
+    return pltpu.make_async_remote_copy(
+        src_ref=src, dst_ref=dst, send_sem=send_sem, recv_sem=recv_sem, device_id=device, device_id_type=MESH
+    )
 
 
 def choice_ranks(routes, experts_all):
@@ -106,14 +26,350 @@
     return jnp.sum(before * onehot, axis=-1).reshape(routes.shape)
 
 
-MESH = pl.DeviceIdType.MESH
-SLOT_ROWS = 8
-
-
-def remote(src, dst, send_sem, recv_sem, device):
-    return pltpu.make_async_remote_copy(
-        src_ref=src, dst_ref=dst, send_sem=send_sem, recv_sem=recv_sem, device_id=device, device_id_type=MESH
-    )
+def attention_kernel(
+    chips_y, q_ref, k_ref, v_ref, bias_ref, gain_ref, w_ref, residual_ref, norm_ref, stream_ref, normed_ref,
+    kv_out, q_out, kv, q_in, gains, weights, acc, carry, att_out, att_in, part, part_out, ring_sum,
+    kv_send, kv_recv, q_send, q_recv, x_send, x_recv, pair_send, pair_recv, w_send, w_recv, g_send, g_recv,
+    att_send, att_recv, rs_send, rs_recv,
+):
+    rows, packed = q_ref.shape
+    size = packed // 2
+    chips_x = lax.axis_size("sp") // chips_y
+    chips = lax.axis_size("tp") // 2
+    width = w_ref.shape[1]
+    far, half = chips // 2, width // 2
+    piece = (pl.ds(0, half), pl.ds(half, half))
+    me, t = lax.axis_index("sp"), lax.axis_index("tp")
+    y, x, z, c = me // chips_x, me % chips_x, t // 2, t % 2
+
+    def device(yy, xx, zz, cc):
+        return (yy * chips_x + xx, 2 * zz + cc)
+
+    def query_core(yy):
+        return ((yy + 1) // 2) % 2
+
+    partner = device(y, x, z, 1 - c)
+    beside = (device(y, (x + 1) % chips_x, z, c), device(y, (x + chips_x - 1) % chips_x, z, c))
+    ahead = (device(y, x, (z + 1) % chips, c), device(y, x, (z + chips - 1) % chips, c))
+    ring = [
+        device((y + dy) % chips_y, x, z, (c + dc) % 2) for dy in range(chips_y) for dc in range(2) if (dy, dc) != (0, 0)
+    ]
+    barrier = pltpu.get_barrier_semaphore()
+    met = [*ring, *beside, *ahead]
+    for other in met:
+        pl.semaphore_signal(barrier, inc=1, device_id=other, device_id_type=MESH)
+
+    empty = jnp.zeros((rows, size), jnp.bfloat16)
+    for h in range(2):
+        lanes = slice(h * size, (h + 1) * size)
+        kv_out[h, pl.ds(0, rows)] = jnp.concatenate([k_ref[:, lanes], v_ref[:, lanes]], axis=1)
+        kv_out[h, pl.ds(rows, 16)] = bias_ref[h]
+        q_out[h] = jnp.concatenate([q_ref[:, lanes] * jnp.bfloat16(-(size ** -0.5)), empty], axis=1)
+    kv[0, pl.ds(0, rows)] = jnp.zeros((rows, packed), jnp.bfloat16)
+    kv[0, pl.ds(rows, 16)] = jnp.full((16, packed), -30000.0, jnp.bfloat16)
+    weights[c] = w_ref[...]
+    gains[c] = gain_ref[...]
+    pl.semaphore_wait(barrier, len(met))
+
+    at_home = (y // 2 == c) & (y % 2 == c)
+    asks_self = (y // 2 == c) & (query_core(y) == c)
+    for h in range(2):
+        j = 2 * c + h
+
+        def kv_remote(h=h, j=j):
+            return remote(kv_out.at[h], kv.at[me + 1], kv_send.at[h], kv_recv.at[y // 2], device(j, x, z, y % 2))
+
+        def q_remote(h=h, j=j):
+            return remote(q_out.at[h], q_in.at[y // 2], q_send.at[h], q_recv.at[y // 2], device(j, x, z, query_core(y)))
+
+        here = at_home & (j == y)
+        asks = asks_self & (j == y)
+        pl.when(jnp.logical_not(here))(lambda f=kv_remote: f().start())
+        pl.when(jnp.logical_not(asks))(lambda f=q_remote: f().start())
+
+        @pl.when(here)
+        def _(h=h):
+            pltpu.make_async_copy(kv_out.at[h], kv.at[me + 1], kv_recv.at[y // 2]).start()
+
+        @pl.when(asks)
+        def _(h=h):
+            pltpu.make_async_copy(q_out.at[h], q_in.at[y // 2], q_recv.at[y // 2]).start()
+
+    to_w = remote(w_ref, weights.at[c], w_send.at[0], w_recv.at[0], partner)
+    to_g = remote(gain_ref, gains.at[c], g_send.at[0], g_recv.at[0], partner)
+    to_g.start()
+
+    def block_at(k, xx):
+        return kv.at[(c + 2 * k) * chips_x + xx + 1]
+
+    def to_partner(k, xx):
+        ref = block_at(k, xx)
+        return remote(ref, ref, pair_send.at[k, xx], pair_recv.at[k, xx], partner)
+
+    def along(d, n, k, xx):
+        ref = block_at(k, xx)
+        return remote(ref, ref, x_send.at[d, n], x_recv.at[d, n], beside[d])
+
+    back_x = ((x + chips_x - 1) % chips_x, (x + 1) % chips_x)
+    across = (x + 2) % chips_x
+    for k in range(2):
+        kept = at_home & (c + 2 * k == y)
+
+        @pl.when(kept)
+        def _(k=k):
+            pltpu.make_async_copy(kv_out.at[0], block_at(k, x), kv_recv.at[k]).wait()
+
+        @pl.when(jnp.logical_not(kept))
+        def _(k=k):
+            remote(kv_out.at[0], block_at(k, x), kv_send.at[0], kv_recv.at[k], partner).wait_recv()
+
+        for d in range(2):
+            along(d, k, k, x).start()
+        to_partner(k, x).start()
+    to_w.start()
+    for d in range(2):
+        along(d, d, d, back_x[d]).wait_recv()
+        along(d, 2, d, back_x[d]).start()
+        to_partner(d, back_x[d]).start()
+    for d in range(2):
+        along(d, 1 - d, 1 - d, back_x[d]).wait_recv()
+        to_partner(1 - d, back_x[d]).start()
+    for d in range(2):
+        along(d, 2, d, across).wait_recv()
+        to_partner(d, across).start()
+    to_g.wait_recv()
+
+    def wait_pair(n, none):
+        k, xx = n // chips_x, n % chips_x
+        ref = kv.at[(1 - c + 2 * k) * chips_x + xx + 1]
+        remote(ref, ref, pair_send.at[k, xx], pair_recv.at[k, xx], partner).wait_recv()
+        return none
+
+    lax.fori_loop(0, 2 * chips_x, wait_pair, 0)
+
+    row = lax.broadcasted_iota(jnp.int32, (CHUNK, CHUNK), 0)
+    col = lax.broadcasted_iota(jnp.int32, (CHUNK, CHUNK), 1)
+    after = (row > col).astype(jnp.bfloat16)
+
+    def attend(slot):
+        from_y = c if slot == 0 else 3 - c
+        block = from_y * chips_x + x
+        asked = asks_self & (from_y == y)
+
+        @pl.when(asked)
+        def _():
+            pltpu.make_async_copy(q_out.at[0], q_in.at[slot], q_recv.at[slot]).wait()
+
+        @pl.when(jnp.logical_not(asked))
+        def _():
+            remote(q_out.at[0], q_in.at[slot], q_send.at[0], q_recv.at[slot], partner).wait_recv()
+
+        acc[...] = jnp.zeros_like(acc)
+        carry[...] = jnp.zeros_like(carry)
+
+        def pair(index, masked):
+            older = block - 2 * index
+
+            def part_of(place, first, length):
+                return kv[older + place, pl.ds(first, length)], kv[older + place, pl.ds(rows, 16)], first // 128, length // 128
+
+            def chunk(sources, place):
+                kv_part = jnp.concatenate([s[0] for s in sources], axis=0)
+                offset = jnp.concatenate(
+                    [s[1][s[2] + n : s[2] + n + 1, :].astype(jnp.float32) for s in sources for n in range(s[3])], axis=1
+                )
+                minus = (
+                    lax.dot_general(
+                        q_in[slot], kv_part, (((1,), (1,)), ((), ())), preferred_element_type=jnp.float32
+                    )
+                    - offset
+                )
+                log_part = jnp.log(1.0 + jnp.exp(-jnp.abs(minus)))
+                drop = jnp.minimum(minus, 0.0) - log_part
+                own_log = drop - minus
+                if masked:
+                    q_at = lax.broadcasted_iota(jnp.int32, (rows, CHUNK), 0) + (rows - place)
+                    earlier = lax.broadcasted_iota(jnp.int32, (rows, CHUNK), 1) < q_at
+                    drop = jnp.where(earlier, drop, 0.0)
+                suffix = jnp.dot(drop.astype(jnp.bfloat16), after, preferred_element_type=jnp.float32)
+                within = jnp.exp(own_log + suffix)
+                if masked:
+                    within = jnp.where(earlier, within, 0.0)
+                product = jnp.dot(within.astype(jnp.bfloat16), kv_part, preferred_element_type=jnp.float32)
+                now = carry[...]
+                acc[...] += jnp.exp(now) * product
+                carry[...] = now + (suffix[:, :1] + drop[:, :1])
+
+            chunk([part_of(1, 128, 256)], 512)
+            chunk([part_of(0, 256, 128), part_of(1, 0, 128)], 256)
+            chunk([part_of(0, 0, 256)], 0)
+
+        pair(0, True)
+
+        def body(index, none):
+            pair(index, False)
+            return none
+
+        lax.fori_loop(1, (block + 2) // 2, body, 0)
+        mixture = acc[...][:, size:]
+        scaled = mixture * lax.rsqrt(jnp.mean(mixture * mixture, axis=-1, keepdims=True) + epsilon)
+        scaled = scaled * gains[y // 2, pl.ds(y % 2, 1), :]
+        by_owner = scaled.reshape(chips, 2, rows // (2 * chips), size)
+        for p in range(2):
+            att_out[slot, p] = by_owner[:, p].astype(jnp.bfloat16)
+            stays = (from_y == y) & (p == c)
+
+            @pl.when(stays)
+            def _(p=p):
+                pltpu.make_async_copy(att_out.at[slot, p], att_in.at[y], att_recv.at[y]).start()
+
+            @pl.when(jnp.logical_not(stays))
+            def _(p=p):
+                send_att(slot, p, from_y).start()
+
+    def send_att(slot, p, from_y):
+        return remote(
+            att_out.at[slot, p], att_in.at[y], att_send.at[slot, p], att_recv.at[y], device(from_y, x, z, p)
+        )
+
+    attend(1)
+    attend(0)
+
+    for j in range(chips_y):
+        stayed = (j == y) & (query_core(y) == c)
+
+        @pl.when(stayed)
+        def _(j=j):
+            pltpu.make_async_copy(att_out.at[0, 0], att_in.at[j], att_recv.at[j]).wait()
+
+        @pl.when(jnp.logical_not(stayed))
+        def _(j=j):
+            remote(att_out.at[0, 0], att_in.at[j], att_send.at[0, 0], att_recv.at[j], partner).wait_recv()
+
+    to_w.wait_recv()
+    heads = [att_in[j].astype(jnp.float32).reshape(rows // 2, size) for j in range(chips_y)]
+    merged = jnp.concatenate(heads, axis=1).astype(jnp.bfloat16)
+    share = jnp.dot(merged, weights[...].reshape(2 * packed, width), preferred_element_type=jnp.float32)
+    part[...] = share.reshape(part.shape)
+
+    def from_sum(d, i, p):
+        ref = ring_sum.at[d, i, :, piece[p]]
+        return remote(ref, ref, rs_send.at[d, i, p], rs_recv.at[d, i, p], ahead[d])
+
+    for i in range(far):
+        for order in range(2):
+            for d in range(2):
+                p = d if order == 0 else 1 - d
+                if i == 0 and p != d:
+                    continue
+                at = ((z + (far - i)) if d == 0 else (z - (far - i) + chips)) % chips
+                total = part[at, :, piece[p]]
+                if i > 1 or (i == 1 and p == d):
+                    from_sum(d, i - 1, p).wait_recv()
+                    total = total + ring_sum[d, i - 1, :, piece[p]].astype(jnp.float32)
+                part_out[d, i, :, piece[p]] = total.astype(jnp.bfloat16)
+                remote(
+                    part_out.at[d, i, :, piece[p]],
+                    ring_sum.at[d, i, :, piece[p]],
+                    rs_send.at[d, i, p],
+                    rs_recv.at[d, i, p],
+                    ahead[d],
+                ).start()
+    for d in range(2):
+        for p in range(2):
+            from_sum(d, far - 1, p).wait_recv()
+    projected = part[z] + ring_sum[0, far - 1].astype(jnp.float32) + ring_sum[1, far - 1].astype(jnp.float32)
+    stream = (residual_ref[...].astype(jnp.float32) + projected).astype(jnp.bfloat16)
+    stream_ref[...] = stream
+    wide = stream.astype(jnp.float32)
+    normed_ref[...] = (
+        wide * lax.rsqrt(jnp.mean(wide * wide, axis=-1, keepdims=True) + epsilon) * norm_ref[...]
+    ).astype(jnp.bfloat16)
+
+    for h in range(2):
+        j = 2 * c + h
+
+        @pl.when(jnp.logical_not(at_home & (j == y)))
+        def _(h=h):
+            remote(kv_out.at[h], kv.at[0], kv_send.at[h], kv_recv.at[0], partner).wait_send()
+
+        @pl.when(jnp.logical_not(asks_self & (j == y)))
+        def _(h=h):
+            remote(q_out.at[h], q_in.at[0], q_send.at[h], q_recv.at[0], partner).wait_send()
+
+    to_w.wait_send()
+    to_g.wait_send()
+    for d in range(2):
+        for n in range(3):
+            along(d, n, 0, x).wait_send()
+
+    def drain_pair(n, none):
+        to_partner(n // chips_x, n % chips_x).wait_send()
+        return none
+
+    lax.fori_loop(0, 2 * chips_x, drain_pair, 0)
+    for slot in range(2):
+        from_y = c if slot == 0 else 3 - c
+        for p in range(2):
+
+            @pl.when(jnp.logical_not((from_y == y) & (p == c)))
+            def _(slot=slot, p=p, from_y=from_y):
+                send_att(slot, p, from_y).wait_send()
+
+    for d in range(2):
+        for i in range(far):
+            for p in range(2):
+                if i > 0 or p == d:
+                    from_sum(d, i, p).wait_send()
+
+
+def attention_layer(queries, keys, values, key_bias, head_gain, out_weight, residual, norm_gain):
+    rows, packed = queries.shape
+    size, width = head_gain.shape[1], out_weight.shape[1]
+    blocks, chips, chips_y = lax.axis_size("sp"), lax.axis_size("tp") // 2, 4
+    chips_x, far, own = blocks // chips_y, chips // 2, residual.shape[0]
+    bias = jnp.pad(key_bias.T.reshape(2, rows // 128, 128), ((0, 0), (0, 16 - rows // 128), (0, 0)))
+    vmem = pl.BlockSpec(memory_space=pltpu.VMEM)
+    bf16, f32, dma = jnp.bfloat16, jnp.float32, pltpu.SemaphoreType.DMA
+    return pl.pallas_call(
+        functools.partial(attention_kernel, chips_y),
+        out_shape=[jax.ShapeDtypeStruct(residual.shape, bf16)] * 2,
+        in_specs=[vmem] * 8,
+        out_specs=[vmem] * 2,
+        scratch_shapes=[
+            pltpu.VMEM((2, rows + 16, packed), bf16),
+            pltpu.VMEM((2, rows, packed), bf16),
+            pltpu.VMEM((blocks + 1, rows + 16, packed), bf16),
+            pltpu.VMEM((2, rows, packed), bf16),
+            pltpu.VMEM((2, 2, size), f32),
+            pltpu.VMEM((2, packed, width), bf16),
+            pltpu.VMEM((rows, packed), f32),
+            pltpu.VMEM((rows, 1), f32),
+            pltpu.VMEM((2, 2, chips, own, size), bf16),
+            pltpu.VMEM((chips_y, chips, own, size), bf16),
+            pltpu.VMEM((chips, own, width), f32),
+            pltpu.VMEM((2, far, own, width), bf16),
+            pltpu.VMEM((2, far, own, width), bf16),
+            dma((2,)),
+            dma((2,)),
+            dma((2,)),
+            dma((2,)),
+            dma((2, 3)),
+            dma((2, 3)),
+            dma((2, chips_x)),
+            dma((2, chips_x)),
+            dma((1,)),
+            dma((1,)),
+            dma((1,)),
+            dma((1,)),
+            dma((2, 2)),
+            dma((chips_y,)),
+            dma((2, far, 2)),
+            dma((2, far, 2)),
+        ],
+        compiler_params=pltpu.CompilerParams(collective_id=2, has_side_effects=True, vmem_limit_bytes=40 << 20),
+        name="attention",
+    )(queries, keys, values, bias, head_gain, out_weight, residual, norm_gain.reshape(1, -1))
 
 
 def expert_kernel(
@@ -502,22 +758,11 @@
     expert_choice,
     expert_weights,
 ):
-    rows_own = queries.shape[0]
-    model_width = out_weight.shape[1]
-    seq_devices = lax.axis_size("sp")
-    head_devices = lax.axis_size("tp")
-    key_piece, value_piece, bias_piece = in_one_piece((keys, values, key_bias), "sp", 0, 1)
-    attended = attention(queries, key_piece, value_piece, bias_piece, head_gain)
-    row_share = rows_own // head_devices
-    merged = lax.all_to_all(attended, "tp", split_axis=0, concat_axis=1, tiled=True)
-    projected = jnp.dot(
-        merged,
-        lax.all_gather(out_weight, "tp", axis=0, tiled=True),
-        preferred_element_type=jnp.float32,
+    seq_devices, head_devices = lax.axis_size("sp"), lax.axis_size("tp")
+    stream, normed = attention_layer(
+        queries, keys, values, key_bias, head_gain, out_weight, residual, norm_gain
     )
-    stream = (residual.astype(jnp.float32) + projected).astype(jnp.bfloat16)
-    normed = (rms_scaled(stream.astype(jnp.float32)) * norm_gain).astype(jnp.bfloat16)
-    cap = 4 * rows_own // (head_devices * seq_devices)
+    cap = 4 * queries.shape[0] // (head_devices * seq_devices)
     return expert_layer(
         stream, normed, expert_choice, expert_weights, gate_proj, up_proj, down_proj, seq_devices, head_devices, cap
     )

time: 245 us -> 174 us (0.71)
  waiting for transfers between devices: 79.1 us -> 0 us
  Pallas kernels: 117 us -> 153 us
  between operations: 13.6 us -> 0.06 us
  starting transfers between devices: 7.17 us -> 0 us
  matrix products: 4.69 us -> 0 us
    all_gather x2 -> x0, waiting for transfers between devices: 76.5 us -> none  [the longest x1 57 us: in_one_piece(): lax.all_gather(both, axis, axis=dim, tiled=True)]
    pallas_call x1, Pallas kernels: 15.8 us -> 50.4 us  [attention_layer(): pl.pallas_call(functools.partial(attention_kernel, chips_y), out_shape=[j...]
    all_to_all x1 -> x0, starting transfers between devices: 7.12 us -> none  [on_device(): lax.all_to_all(attended, 'tp', split_axis=0, concat_axis=1, tiled=True)]
    dot_general x1 -> x0, matrix products: 4.69 us -> none  [on_device(): jnp.dot(merged, lax.all_gather(out_weight, 'tp', axis=0, tiled=True), pre...]
    split x1 -> x0, local copies, waits for them, and re-layouts: 3.36 us -> none  [in_one_piece(): jnp.split(lax.all_gather(both, axis, axis=dim, tiled=True), ends, axis=al...]
    unnamed x22 -> x24, local copies, waits for them, and re-layouts: 13.5 us -> 16 us
  transfers between devices with their start and end apart: 3 -> 0, of which waited for: 3 -> 0; matrix products, arithmetic and copies ran while one was open for 7% -> 0% of each run, Pallas kernels for 6% -> 0%
where the time goes in v3:
time: 174 us
  Pallas kernels  153 us (88%)
  local copies, waits for them, and re-layouts  17.7 us (10%)
  other arithmetic  2.47 us (1%)
    pallas_call x1, Pallas kernels, expert_layer(): pl.pallas_call(functools.partial(expert_kernel, cap), out_shape=jax.Shape...  103 us
    pallas_call x1, Pallas kernels, attention_layer(): pl.pallas_call(functools.partial(attention_kernel, chips_y), out_shape=[j...  50.4 us
    unnamed x24, local copies, waits for them, and re-layouts  16 us

profile of v3, /device:TPU:24, one launch (start us, length us, event | category | flops | bytes accessed | tf_op | source)
XLA Modules:
  0.0 173.5 jit_solution(15429218932034689300)
XLA Ops:
  0.0 0.7 reshape.12
  0.7 0.8 copy.33
  1.5 0.1 eq.28
  1.6 0.1 reduce_window_sum.11
  1.7 0.2 select_reduce_fusion.1
  1.9 0.1 reshape.14
  2.0 0.1 copy.34
  2.1 0.7 multiply_add_fusion
  2.9 1.4 select_reduce_fusion.weight_ref
  4.2 0.7 copy.35
  4.9 1.0 copy-done
  6.0 0.9 copy-done.1
  6.9 0.9 copy-done.2
  7.8 0.9 copy-done.3
  8.7 0.9 copy-done.4
  9.5 0.7 copy-done.7
  10.2 0.7 copy-done.8
  10.9 50.4 %attention.1 = (bf16[24,2048]{1,0:T(8,128)(2,1)S(1)}, bf16[24,2048]{1,0:T(8,128)(2,1)S(1)}) custom-call(bf16[384,128]{1,0:T(8,128)(2,1)S(1)} %copy-done.1, bf16[384,128]{1,0:T(8,128)(2,1)S(1)} %copy-done.2, bf16[384,128]{1,0:T(8,128)(2,1)S(1)} %copy-done.3, bf16[2,16,128]{2,1,0:T(8,128)(2,1)S(1)} %pad.4.bias_ref, f32[2,64]{1,0:T(2,128)S(1)} %copy-done.8, ...), custom_call_target="tpu_custom_call" | custom-call | tf_op jit(solution)/shard_map/attention/pallas_call | solution.py:334
  61.3 0.6 copy-done.5
  62.0 0.6 copy-done.6
  62.6 4.0 %copy.36.gate_hbm = bf16[1,2048,448]{2,1,0:T(8,128)(2,1)} copy(bf16[1,2048,448]{1,2,0:T(8,128)(2,1)} %param.21) | data formatting | bytes 3670016 | tf_op args[8]
  66.6 2.5 %copy.37.up_hbm = bf16[1,2048,448]{2,1,0:T(8,128)(2,1)} copy(bf16[1,2048,448]{1,2,0:T(8,128)(2,1)S(1)} %copy-done.9) | data formatting | bytes 3670016 | tf_op args[9]
  69.0 102.9 %experts.1 = bf16[24,2048]{1,0:T(8,128)(2,1)} custom-call(bf16[24,2048]{1,0:T(8,128)(2,1)} %copy-done.5, bf16[24,2048]{1,0:T(8,128)(2,1)} %copy-done.6, bf16[128,24]{1,0:T(8,128)(2,1)} %bitcast.4, f32[24,128]{1,0:T(8,128)} %select_reduce_fusion.weight_ref, bf16[1,2048,448]{2,1,0:T(8,128)(2,1)} %copy.36.gate_hbm, bf16[1,2048,448]{2,1,0:T(8,128)(2,1)} %copy.37.up_hbm, ...), custom_call_target="tpu_custom_call" | custom-call | tf_op jit(solution)/shard_map/experts/pallas_call | solution.py:708
  172.0 1.5 copy.39
  (15 shorter events, 0.2 us)
Async XLA Ops:
  4.9 1.0 copy-start
  6.0 0.9 copy-start.1
  6.9 0.9 copy-start.2
  7.8 0.9 copy-start.3
  8.7 0.9 copy-start.4
  9.5 0.7 copy-start.7
  10.2 0.7 copy-start.8
  61.3 0.6 copy-start.5
  62.0 0.6 copy-start.6
  62.6 4.0 %copy-start.9 = (bf16[1,2048,448]{1,2,0:T(8,128)(2,1)S(1)}, bf16[1,2048,448]{1,2,0:T(8,128)(2,1)}, u32[]{:S(2)}) copy-start(bf16[1,2048,448]{1,2,0:T(8,128)(2,1)} %param.22) | copy-start | bytes 5505028

commit v4 on v3

--- a/solution.py
+++ b/solution.py
@@ -19,16 +19,9 @@
     )
 
 
-def choice_ranks(routes, experts_all):
-    flat_routes = routes.reshape(routes.shape[:-2] + (-1,))
-    onehot = (flat_routes[..., None] == jnp.arange(experts_all, dtype=jnp.int32)).astype(jnp.int32)
-    before = jnp.cumsum(onehot, axis=-2) - onehot
-    return jnp.sum(before * onehot, axis=-1).reshape(routes.shape)
-
-
-def attention_kernel(
-    chips_y, q_ref, k_ref, v_ref, bias_ref, gain_ref, w_ref, residual_ref, norm_ref, stream_ref, normed_ref,
-    kv_out, q_out, kv, q_in, gains, weights, acc, carry, att_out, att_in, part, part_out, ring_sum,
+def attention_part(
+    chips_y, loads, route, q_ref, k_ref, v_ref, bias_ref, gain_ref, w_ref, residual_ref, norm_ref, stream_ref, normed_ref,
+    kv_out, q_out, kv, q_in, q_wide, gains, weights, acc, carry, att_out, att_in, part, part_out, ring_sum,
     kv_send, kv_recv, q_send, q_recv, x_send, x_recv, pair_send, pair_recv, w_send, w_recv, g_send, g_recv,
     att_send, att_recv, rs_send, rs_recv,
 ):
@@ -51,53 +44,62 @@
     partner = device(y, x, z, 1 - c)
     beside = (device(y, (x + 1) % chips_x, z, c), device(y, (x + chips_x - 1) % chips_x, z, c))
     ahead = (device(y, x, (z + 1) % chips, c), device(y, x, (z + chips - 1) % chips, c))
-    ring = [
-        device((y + dy) % chips_y, x, z, (c + dc) % 2) for dy in range(chips_y) for dc in range(2) if (dy, dc) != (0, 0)
-    ]
     barrier = pltpu.get_barrier_semaphore()
-    met = [*ring, *beside, *ahead]
-    for other in met:
+    sources = lax.axis_size("sp")
+
+    def greet(n, none):
+        pl.semaphore_signal(barrier, inc=1, device_id=((me + n) % sources, t), device_id_type=MESH)
+        return none
+
+    lax.fori_loop(1, sources, greet, 0)
+    others = [device((y + dy) % chips_y, x, z, 1 - c) for dy in range(chips_y)] + list(ahead)
+    for other in others:
         pl.semaphore_signal(barrier, inc=1, device_id=other, device_id_type=MESH)
-
-    empty = jnp.zeros((rows, size), jnp.bfloat16)
+    for load in loads[:5]:
+        load.wait()
+
+    offsets = bias_ref[...].astype(jnp.float32)
     for h in range(2):
         lanes = slice(h * size, (h + 1) * size)
         kv_out[h, pl.ds(0, rows)] = jnp.concatenate([k_ref[:, lanes], v_ref[:, lanes]], axis=1)
-        kv_out[h, pl.ds(rows, 16)] = bias_ref[h]
-        q_out[h] = jnp.concatenate([q_ref[:, lanes] * jnp.bfloat16(-(size ** -0.5)), empty], axis=1)
+        by_row = [offsets[h : h + 1, n * packed : (n + 1) * packed] for n in range(rows // packed)]
+        by_row.append(jnp.zeros((16 - rows // packed, packed), jnp.float32))
+        kv_out[h, pl.ds(rows, 16)] = jnp.concatenate(by_row, axis=0).astype(jnp.bfloat16)
+        q_neg = q_ref[:, lanes] * jnp.bfloat16(-(size ** -0.5))
+        q_out[h] = jnp.concatenate([q_neg[: rows // 2], q_neg[rows // 2 :]], axis=1)
     kv[0, pl.ds(0, rows)] = jnp.zeros((rows, packed), jnp.bfloat16)
     kv[0, pl.ds(rows, 16)] = jnp.full((16, packed), -30000.0, jnp.bfloat16)
-    weights[c] = w_ref[...]
     gains[c] = gain_ref[...]
-    pl.semaphore_wait(barrier, len(met))
+    pl.semaphore_wait(barrier, sources - 1 + len(others))
 
     at_home = (y // 2 == c) & (y % 2 == c)
     asks_self = (y // 2 == c) & (query_core(y) == c)
     for h in range(2):
         j = 2 * c + h
 
-        def kv_remote(h=h, j=j):
-            return remote(kv_out.at[h], kv.at[me + 1], kv_send.at[h], kv_recv.at[y // 2], device(j, x, z, y % 2))
-
-        def q_remote(h=h, j=j):
-            return remote(q_out.at[h], q_in.at[y // 2], q_send.at[h], q_recv.at[y // 2], device(j, x, z, query_core(y)))
-
-        here = at_home & (j == y)
-        asks = asks_self & (j == y)
-        pl.when(jnp.logical_not(here))(lambda f=kv_remote: f().start())
-        pl.when(jnp.logical_not(asks))(lambda f=q_remote: f().start())
-
-        @pl.when(here)
+        @pl.when(jnp.logical_not(at_home & (j == y)))
+        def _(h=h, j=j):
+            remote(kv_out.at[h], kv.at[me + 1], kv_send.at[h], kv_recv.at[y // 2], device(j, x, z, y % 2)).start()
+
+        @pl.when(at_home & (j == y))
         def _(h=h):
             pltpu.make_async_copy(kv_out.at[h], kv.at[me + 1], kv_recv.at[y // 2]).start()
 
-        @pl.when(asks)
+    for h in range(2):
+        j = 2 * c + h
+
+        @pl.when(jnp.logical_not(asks_self & (j == y)))
+        def _(h=h, j=j):
+            remote(q_out.at[h], q_in.at[y // 2], q_send.at[h], q_recv.at[y // 2], device(j, x, z, query_core(y))).start()
+
+        @pl.when(asks_self & (j == y))
         def _(h=h):
             pltpu.make_async_copy(q_out.at[h], q_in.at[y // 2], q_recv.at[y // 2]).start()
 
     to_w = remote(w_ref, weights.at[c], w_send.at[0], w_recv.at[0], partner)
     to_g = remote(gain_ref, gains.at[c], g_send.at[0], g_recv.at[0], partner)
     to_g.start()
+    route()
 
     def block_at(k, xx):
         return kv.at[(c + 2 * k) * chips_x + xx + 1]
@@ -126,7 +128,10 @@
         for d in range(2):
             along(d, k, k, x).start()
         to_partner(k, x).start()
+    for load in loads[5:]:
+        load.wait()
     to_w.start()
+    weights[c] = w_ref[...]
     for d in range(2):
         along(d, d, d, back_x[d]).wait_recv()
         along(d, 2, d, back_x[d]).start()
@@ -164,6 +169,9 @@
         def _():
             remote(q_out.at[0], q_in.at[slot], q_send.at[0], q_recv.at[slot], partner).wait_recv()
 
+        folded = q_in[slot]
+        q_here = jnp.concatenate([folded[:, :size], folded[:, size:]], axis=0)
+        q_wide[...] = jnp.concatenate([q_here, jnp.zeros_like(q_here)], axis=1)
         acc[...] = jnp.zeros_like(acc)
         carry[...] = jnp.zeros_like(carry)
 
@@ -180,7 +188,7 @@
                 )
                 minus = (
                     lax.dot_general(
-                        q_in[slot], kv_part, (((1,), (1,)), ((), ())), preferred_element_type=jnp.float32
+                        q_wide[...], kv_part, (((1,), (1,)), ((), ())), preferred_element_type=jnp.float32
                     )
                     - offset
                 )
@@ -323,59 +331,10 @@
                     from_sum(d, i, p).wait_send()
 
 
-def attention_layer(queries, keys, values, key_bias, head_gain, out_weight, residual, norm_gain):
-    rows, packed = queries.shape
-    size, width = head_gain.shape[1], out_weight.shape[1]
-    blocks, chips, chips_y = lax.axis_size("sp"), lax.axis_size("tp") // 2, 4
-    chips_x, far, own = blocks // chips_y, chips // 2, residual.shape[0]
-    bias = jnp.pad(key_bias.T.reshape(2, rows // 128, 128), ((0, 0), (0, 16 - rows // 128), (0, 0)))
-    vmem = pl.BlockSpec(memory_space=pltpu.VMEM)
-    bf16, f32, dma = jnp.bfloat16, jnp.float32, pltpu.SemaphoreType.DMA
-    return pl.pallas_call(
-        functools.partial(attention_kernel, chips_y),
-        out_shape=[jax.ShapeDtypeStruct(residual.shape, bf16)] * 2,
-        in_specs=[vmem] * 8,
-        out_specs=[vmem] * 2,
-        scratch_shapes=[
-            pltpu.VMEM((2, rows + 16, packed), bf16),
-            pltpu.VMEM((2, rows, packed), bf16),
-            pltpu.VMEM((blocks + 1, rows + 16, packed), bf16),
-            pltpu.VMEM((2, rows, packed), bf16),
-            pltpu.VMEM((2, 2, size), f32),
-            pltpu.VMEM((2, packed, width), bf16),
-            pltpu.VMEM((rows, packed), f32),
-            pltpu.VMEM((rows, 1), f32),
-            pltpu.VMEM((2, 2, chips, own, size), bf16),
-            pltpu.VMEM((chips_y, chips, own, size), bf16),
-            pltpu.VMEM((chips, own, width), f32),
-            pltpu.VMEM((2, far, own, width), bf16),
-            pltpu.VMEM((2, far, own, width), bf16),
-            dma((2,)),
-            dma((2,)),
-            dma((2,)),
-            dma((2,)),
-            dma((2, 3)),
-            dma((2, 3)),
-            dma((2, chips_x)),
-            dma((2, chips_x)),
-            dma((1,)),
-            dma((1,)),
-            dma((1,)),
-            dma((1,)),
-            dma((2, 2)),
-            dma((chips_y,)),
-            dma((2, far, 2)),
-            dma((2, far, 2)),
-        ],
-        compiler_params=pltpu.CompilerParams(collective_id=2, has_side_effects=True, vmem_limit_bytes=40 << 20),
-        name="attention",
-    )(queries, keys, values, bias, head_gain, out_weight, residual, norm_gain.reshape(1, -1))
-
-
-def expert_kernel(
-    cap, stream_ref, normed_ref, select_ref, weight_ref, gate_hbm, up_hbm, down_hbm, out_ref,
-    outgoing, arrived, rows, part, partner_part, ring_sum, back, returned, gate_w, up_w, down_w,
-    load_sem, go_send, go_recv, ag_send, ag_recv, pair_send, pair_recv, pin_send, pin_recv,
+def expert_part(
+    cap, loads, gate_w, up_w, down_w, stream_ref, normed_ref, select_ref, weight_ref, out_ref,
+    outgoing, arrived, rows, part, partner_part, ring_sum, back, returned,
+    go_send, go_recv, ag_send, ag_recv, pair_send, pair_recv, pin_send, pin_recv,
     rs_send, rs_recv, back_send, back_recv,
 ):
     experts, _, width = outgoing.shape
@@ -387,27 +346,11 @@
     ahead = ((me, 2 * ((z + 1) % chips) + c), (me, 2 * ((z + chips - 1) % chips) + c))
     piece = (pl.ds(0, half), pl.ds(half, half))
 
-    barrier = pltpu.get_barrier_semaphore()
-    for device in (partner, *ahead):
-        pl.semaphore_signal(barrier, inc=1, device_id=device, device_id_type=MESH)
-
-    def greet(j, none):
-        pl.semaphore_signal(barrier, inc=1, device_id=((me + j) % experts, t), device_id_type=MESH)
-        return none
-
-    lax.fori_loop(1, experts, greet, 0)
-    loads = [
-        pltpu.make_async_copy(src.at[0], dst, load_sem.at[i])
-        for i, (src, dst) in enumerate(((gate_hbm, gate_w), (up_hbm, up_w), (down_hbm, down_w)))
-    ]
-    for load in loads:
-        load.start()
     chosen = jnp.dot(select_ref[...], normed_ref[...], preferred_element_type=jnp.float32)
     outgoing[...] = chosen.reshape(experts, SLOT_ROWS, width).astype(jnp.bfloat16)
     for k in range(chunks):
         for d in range(2):
             ring_sum[k, d, 0, :, piece[1 - d]] = jnp.zeros((block, half), jnp.bfloat16)
-    pl.semaphore_wait(barrier, experts + 2)
 
     def go(src, dst, source_id, device):
         return remote(src, dst, go_send.at[source_id], go_recv.at[source_id], device)
@@ -500,8 +443,9 @@
     def experts_on(k, i):
         at = pl.ds(i * group, group)
         x = rows[k, at].reshape(group * 2 * block, width)
-        gate = jnp.dot(x, gate_w[...], preferred_element_type=jnp.float32)
-        up = jnp.dot(x, up_w[...], preferred_element_type=jnp.float32)
+        across = (((1,), (1,)), ((), ()))
+        gate = lax.dot_general(x, gate_w[...], across, preferred_element_type=jnp.float32)
+        up = lax.dot_general(x, up_w[...], across, preferred_element_type=jnp.float32)
         hidden = (gate / (1.0 + jnp.exp(-gate)) * up).astype(jnp.bfloat16)
         product = jnp.dot(hidden, down_w[...], preferred_element_type=jnp.float32)
         part[k, at] = product.astype(jnp.bfloat16).reshape(group, 2, block, width)
@@ -641,15 +585,12 @@
         return none
 
     lax.fori_loop(0, experts, wait_back, 0)
-    weights = weight_ref[...]
-    high = weights.astype(jnp.bfloat16)
-    rest = weights - high.astype(jnp.float32)
-    middle = rest.astype(jnp.bfloat16)
-    low = (rest - middle.astype(jnp.float32)).astype(jnp.bfloat16)
     picked = returned[...].astype(jnp.float32).reshape(experts * SLOT_ROWS, width).astype(jnp.bfloat16)
     combined = stream_ref[...].astype(jnp.float32)
-    for share in (low, middle, high):
-        combined = combined + jnp.dot(share, picked, preferred_element_type=jnp.float32)
+    for n in reversed(range(3)):
+        combined = combined + lax.dot_general(
+            weight_ref[n], picked, (((0,), (0,)), ((), ())), preferred_element_type=jnp.float32
+        )
     out_ref[...] = combined.astype(jnp.bfloat16)
 
     def drain_sp(j, none):
@@ -693,79 +634,136 @@
     lax.fori_loop(0, far, drain_ring, 0)
 
 
-def expert_layer(stream, normed, choice, choice_weights, gate_proj, up_proj, down_proj, seq_devices, head_devices, cap):
-    own_rows, width = stream.shape
-    hidden = gate_proj.shape[2]
-    experts, chips, chunks = seq_devices, head_devices // 2, 2
-    far, block = chips // 2, seq_devices // chunks * cap
-    slots = choice * SLOT_ROWS + choice_ranks(choice, experts)
-    targets = jnp.arange(experts * SLOT_ROWS, dtype=jnp.int32)
-    match = slots[:, :, None] == targets[None, None, :]
-    select = jnp.any(match, axis=1).T.astype(jnp.bfloat16)
-    weights = jnp.sum(jnp.where(match, choice_weights[:, :, None], 0.0), axis=1)
-    vmem, hbm = pl.BlockSpec(memory_space=pltpu.VMEM), pl.BlockSpec(memory_space=pl.ANY)
-    bf16, dma = jnp.bfloat16, pltpu.SemaphoreType.DMA
+def layer_kernel(
+    chips_y, cap, q_hbm, k_hbm, v_hbm, bias_hbm, gain_hbm, w_hbm, residual_hbm, norm_hbm, choice_hbm, share_hbm,
+    gate_hbm, up_hbm, down_hbm, out_ref, q, k, v, bias, gain, w, residual, norm, choice, share, gate_w, up_w, down_w,
+    load_sem, stream, normed, select, weight, *scratch,
+):
+    sources = (q_hbm, k_hbm, v_hbm, bias_hbm, gain_hbm, w_hbm, residual_hbm, norm_hbm, choice_hbm, share_hbm)
+    sources += (gate_hbm.at[0], up_hbm.at[0], down_hbm.at[0])
+    places = (q, k, v, bias, gain, w, residual, norm, choice, share, gate_w, up_w, down_w)
+    loads = [pltpu.make_async_copy(src, dst, load_sem.at[i]) for i, (src, dst) in enumerate(zip(sources, places))]
+    for load in loads:
+        load.start()
+
+    def route():
+        for load in loads[8:10]:
+            load.wait()
+        slots, own_rows = select.shape
+        slot = lax.broadcasted_iota(jnp.int32, (slots, own_rows), 0)
+        expert, place = slot // SLOT_ROWS, slot % SLOT_ROWS
+        first = choice[0:1, :] == expert
+        named = first | (choice[1:2, :] == expert)
+        earlier = lax.broadcasted_iota(jnp.int32, (own_rows, own_rows), 0) < lax.broadcasted_iota(
+            jnp.int32, (own_rows, own_rows), 1
+        )
+        before = jnp.dot(
+            named.astype(jnp.bfloat16), earlier.astype(jnp.bfloat16), preferred_element_type=jnp.float32
+        )
+        chosen = named & (before.astype(jnp.int32) == place)
+        select[...] = chosen.astype(jnp.bfloat16)
+        rest = jnp.where(chosen, jnp.where(first, share[0:1, :], share[1:2, :]), 0.0)
+        for n in range(3):
+            term = rest.astype(jnp.bfloat16)
+            weight[n] = term
+            rest = rest - term.astype(jnp.float32)
+
+    attention_part(
+        chips_y, loads[:8], route, q, k, v, bias, gain, w, residual, norm, stream, normed, *scratch[:ATTENTION_SCRATCH]
+    )
+    expert_part(cap, loads[10:], gate_w, up_w, down_w, stream, normed, select, weight, out_ref, *scratch[ATTENTION_SCRATCH:])
+
+
+ATTENTION_SCRATCH = 30
+
+
+def layer(
+    queries, keys, values, key_bias, head_gain, out_weight, residual, norm_gain, gate_proj, up_proj, down_proj,
+    expert_choice, expert_weights,
+):
+    rows, packed = queries.shape
+    size, width, hidden = head_gain.shape[1], out_weight.shape[1], gate_proj.shape[2]
+    blocks, chips, chips_y, chunks = lax.axis_size("sp"), lax.axis_size("tp") // 2, 4, 2
+    chips_x, far, own = blocks // chips_y, chips // 2, residual.shape[0]
+    cap = 4 * own // blocks
+    block, slots = blocks // chunks * cap, blocks * SLOT_ROWS
+    bf16, f32, dma = jnp.bfloat16, jnp.float32, pltpu.SemaphoreType.DMA
+    arguments = (
+        queries, keys, values, key_bias.T, head_gain, out_weight, residual, norm_gain.reshape(1, -1),
+        expert_choice.T, expert_weights.T, gate_proj.swapaxes(1, 2), up_proj.swapaxes(1, 2), down_proj,
+    )
+    scratch = [pltpu.VMEM(a.shape[-2:], a.dtype) for a in arguments]
+    scratch += [
+        dma((len(arguments),)),
+        pltpu.VMEM((own, width), bf16),
+        pltpu.VMEM((own, width), bf16),
+        pltpu.VMEM((slots, own), bf16),
+        pltpu.VMEM((3, slots, own), bf16),
+    ]
+    attention_scratch = [
+        pltpu.VMEM((2, rows + 16, packed), bf16),
+        pltpu.VMEM((2, rows // 2, packed), bf16),
+        pltpu.VMEM((blocks + 1, rows + 16, packed), bf16),
+        pltpu.VMEM((2, rows // 2, packed), bf16),
+        pltpu.VMEM((rows, packed), bf16),
+        pltpu.VMEM((2, 2, size), f32),
+        pltpu.VMEM((2, packed, width), bf16),
+        pltpu.VMEM((rows, packed), f32),
+        pltpu.VMEM((rows, 1), f32),
+        pltpu.VMEM((2, 2, chips, own, size), bf16),
+        pltpu.VMEM((chips_y, chips, own, size), bf16),
+        pltpu.VMEM((chips, own, width), f32),
+        pltpu.VMEM((2, far, own, width), bf16),
+        pltpu.VMEM((2, far, own, width), bf16),
+        dma((2,)),
+        dma((2,)),
+        dma((2,)),
+        dma((2,)),
+        dma((2, 3)),
+        dma((2, 3)),
+        dma((2, chips_x)),
+        dma((2, chips_x)),
+        dma((1,)),
+        dma((1,)),
+        dma((1,)),
+        dma((1,)),
+        dma((2, 2)),
+        dma((chips_y,)),
+        dma((2, far, 2)),
+        dma((2, far, 2)),
+    ]
+    expert_scratch = [
+        pltpu.VMEM((blocks, SLOT_ROWS, width), bf16),
+        pltpu.VMEM((blocks, SLOT_ROWS, width), bf16),
+        pltpu.VMEM((chunks, chips, 2, block, width), bf16),
+        pltpu.VMEM((chunks, chips, 2, block, width), bf16),
+        pltpu.VMEM((chunks, chips, block, width), bf16),
+        pltpu.VMEM((chunks, 2, far, block, width), bf16),
+        pltpu.VMEM((blocks, SLOT_ROWS, width), bf16),
+        pltpu.VMEM((blocks, SLOT_ROWS, width), bf16),
+        dma((blocks,)),
+        dma((blocks,)),
+        dma((chunks, 2, far, 2)),
+        dma((chunks, 2, far, 2)),
+        dma((chunks, chips, 2)),
+        dma((chunks, chips, 2)),
+        dma((chunks, chips)),
+        dma((chunks, chips)),
+        dma((chunks, 2, far, 2)),
+        dma((chunks, 2, far, 2)),
+        dma((blocks,)),
+        dma((blocks,)),
+    ]
+    assert len(attention_scratch) == ATTENTION_SCRATCH
     return pl.pallas_call(
-        functools.partial(expert_kernel, cap),
-        out_shape=jax.ShapeDtypeStruct(stream.shape, bf16),
-        in_specs=[vmem] * 4 + [hbm] * 3,
-        out_specs=vmem,
-        scratch_shapes=[
-            pltpu.VMEM((experts, SLOT_ROWS, width), bf16),
-            pltpu.VMEM((experts, SLOT_ROWS, width), bf16),
-            pltpu.VMEM((chunks, chips, 2, block, width), bf16),
-            pltpu.VMEM((chunks, chips, 2, block, width), bf16),
-            pltpu.VMEM((chunks, chips, block, width), bf16),
-            pltpu.VMEM((chunks, 2, far, block, width), bf16),
-            pltpu.VMEM((experts, SLOT_ROWS, width), bf16),
-            pltpu.VMEM((experts, SLOT_ROWS, width), bf16),
-            pltpu.VMEM((width, hidden), bf16),
-            pltpu.VMEM((width, hidden), bf16),
-            pltpu.VMEM((hidden, width), bf16),
-            dma((3,)),
-            dma((experts,)),
-            dma((experts,)),
-            dma((chunks, 2, far, 2)),
-            dma((chunks, 2, far, 2)),
-            dma((chunks, chips, 2)),
-            dma((chunks, chips, 2)),
-            dma((chunks, chips)),
-            dma((chunks, chips)),
-            dma((chunks, 2, far, 2)),
-            dma((chunks, 2, far, 2)),
-            dma((experts,)),
-            dma((experts,)),
-        ],
-        compiler_params=pltpu.CompilerParams(
-            collective_id=1, has_side_effects=True, vmem_limit_bytes=56 << 20
-        ),
-        name="experts",
-    )(stream, normed, select, weights, gate_proj, up_proj, down_proj)
-
-
-def on_device(
-    queries,
-    keys,
-    values,
-    key_bias,
-    head_gain,
-    out_weight,
-    residual,
-    norm_gain,
-    gate_proj,
-    up_proj,
-    down_proj,
-    expert_choice,
-    expert_weights,
-):
-    seq_devices, head_devices = lax.axis_size("sp"), lax.axis_size("tp")
-    stream, normed = attention_layer(
-        queries, keys, values, key_bias, head_gain, out_weight, residual, norm_gain
-    )
-    cap = 4 * queries.shape[0] // (head_devices * seq_devices)
-    return expert_layer(
-        stream, normed, expert_choice, expert_weights, gate_proj, up_proj, down_proj, seq_devices, head_devices, cap
-    )
+        functools.partial(layer_kernel, chips_y, cap),
+        out_shape=jax.ShapeDtypeStruct(residual.shape, bf16),
+        in_specs=[pl.BlockSpec(memory_space=pl.ANY)] * len(arguments),
+        out_specs=pl.BlockSpec(memory_space=pltpu.VMEM),
+        scratch_shapes=scratch + attention_scratch + expert_scratch,
+        compiler_params=pltpu.CompilerParams(collective_id=1, has_side_effects=True, vmem_limit_bytes=60 << 20),
+        name="layer",
+    )(*arguments)
 
 
 def solution(mesh):
@@ -785,5 +783,5 @@
         P(("sp", "tp"), None),
     )
     return jax.shard_map(
-        on_device, mesh=mesh, in_specs=placed, out_specs=P(("sp", "tp"), None), check_vma=False
+        layer, mesh=mesh, in_specs=placed, out_specs=P(("sp", "tp"), None), check_vma=False
     )

time: 174 us -> 154 us (0.89)
  local copies, waits for them, and re-layouts: 17.7 us -> 1.54 us
  other arithmetic: 2.47 us -> 0 us
    unnamed x24 -> x1, local copies, waits for them, and re-layouts: 16 us -> 1.54 us
    pallas_call x2 -> x1, Pallas kernels: 153 us -> 153 us  [layer(): pl.pallas_call(functools.partial(layer_kernel, chips_y, cap), out_shape=j...]
where the time goes in v4:
time: 154 us
  Pallas kernels  153 us (99%)
  local copies, waits for them, and re-layouts  1.54 us (1%)
    pallas_call x1, Pallas kernels, layer(): pl.pallas_call(functools.partial(layer_kernel, chips_y, cap), out_shape=j...  153 us

profile of v4, /device:TPU:24, one launch (start us, length us, event | category | flops | bytes accessed | tf_op | source)
XLA Modules:
  0.0 154.1 jit_solution(10801814681179309363)
XLA Ops:
  0.0 152.6 %layer.1 = bf16[24,2048]{1,0:T(8,128)(2,1)} custom-call(bf16[384,128]{1,0:T(8,128)(2,1)} %q_hbm.1, bf16[384,128]{1,0:T(8,128)(2,1)} %k_hbm.1, bf16[384,128]{1,0:T(8,128)(2,1)} %v_hbm.1, bf16[2,384]{1,0:T(2,128)(2,1)} %bitcast.9, f32[2,64]{1,0:T(2,128)} %gain_hbm.1, bf16[128,2048]{1,0:T(8,128)(2,1)} %w_hbm.1, bf16[24,2048]{1,0:T(8,128)(2,1)} %residual_hbm.1, ...), custom_call_target="tpu_custom_call" | custom-call | tf_op jit(solution)/shard_map/layer/pallas_call | solution.py:758
  152.6 1.5 copy.15

commit v5 on v4

v5 whole, which is shorter than its diff:
```python
import functools

import jax
import jax.numpy as jnp
from jax import lax
from jax.experimental import pallas as pl
from jax.experimental.pallas import tpu as pltpu
from jax.sharding import PartitionSpec as P

epsilon = 1e-06
CHUNK = 256
MESH = pl.DeviceIdType.MESH
SLOT_ROWS = 8


def remote(src, dst, send_sem, recv_sem, device):
    return pltpu.make_async_remote_copy(
        src_ref=src, dst_ref=dst, send_sem=send_sem, recv_sem=recv_sem, device_id=device, device_id_type=MESH
    )


def attention_part(
    chips_y, loads, route, q_ref, k_ref, v_ref, bias_ref, gain_ref, w_ref, residual_ref, norm_ref, stream_ref, normed_ref,
    kv_out, q_out, kv, q_in, q_wide, gains, weights, acc, carry, early, early_carry, att_out, att_in, part, part_out, ring_sum,
    kv_send, kv_recv, q_send, q_recv, pair_send, pair_recv, w_send, w_recv, g_send, g_recv,
    att_send, att_recv, rs_send, rs_recv,
):
    rows, packed = q_ref.shape
    size = packed // 2
    chips_x = lax.axis_size("sp") // chips_y
    chips = lax.axis_size("tp") // 2
    width = w_ref.shape[1]
    far, half = chips // 2, width // 2
    quarter = [pl.ds(n * half // 2, half // 2) for n in range(4)]
    me, t = lax.axis_index("sp"), lax.axis_index("tp")
    y, x, z, c = me // chips_x, me % chips_x, t // 2, t % 2

    def device(yy, xx, zz, cc):
        return (yy * chips_x + xx, 2 * zz + cc)

    def query_core(yy):
        return ((yy + 1) // 2) % 2

    partner = device(y, x, z, 1 - c)
    ahead = (device(y, x, (z + 1) % chips, c), device(y, x, (z + chips - 1) % chips, c))
    barrier = pltpu.get_barrier_semaphore()
    sources = lax.axis_size("sp")

    def greet(n, none):
        pl.semaphore_signal(barrier, inc=1, device_id=((me + n) % sources, t), device_id_type=MESH)
        return none

    lax.fori_loop(1, sources, greet, 0)
    others = [device((y + dy) % chips_y, x, z, 1 - c) for dy in range(chips_y)] + list(ahead)
    for other in others:
        pl.semaphore_signal(barrier, inc=1, device_id=other, device_id_type=MESH)
    for load in loads[:5]:
        load.wait()

    offsets = bias_ref[...].astype(jnp.float32)
    for h in range(2):
        lanes = slice(h * size, (h + 1) * size)
        kv_out[h, pl.ds(0, rows)] = jnp.concatenate([k_ref[:, lanes], v_ref[:, lanes]], axis=1)
        by_row = [offsets[h : h + 1, n * packed : (n + 1) * packed] for n in range(rows // packed)]
        by_row.append(jnp.zeros((16 - rows // packed, packed), jnp.float32))
        kv_out[h, pl.ds(rows, 16)] = jnp.concatenate(by_row, axis=0).astype(jnp.bfloat16)
        q_neg = q_ref[:, lanes] * jnp.bfloat16(-(size ** -0.5))
        q_out[h] = jnp.concatenate([q_neg[: rows // 2], q_neg[rows // 2 :]], axis=1)
    gains[c] = gain_ref[...]
    pl.semaphore_wait(barrier, sources - 1 + len(others))

    keeper = y // 2 == c
    asks_self = keeper & (query_core(y) == c)
    side, base = x % 2, x // 2 * 2
    other = (base + 2) % chips_x
    columns = (x, base + 1 - side, other + 1 - side, other + side)

    def to_column(h, n):
        return remote(
            kv_out.at[h], kv.at[me], kv_send.at[h, n], kv_recv.at[me], device(2 * c + h, columns[n], z, c)
        )

    for n in range(4):
        for h in range(2):
            if n > 0:
                to_column(h, n).start()
            else:
                pl.when(jnp.logical_not(2 * c + h == y))(lambda h=h: to_column(h, 0).start())

                @pl.when(2 * c + h == y)
                def _(h=h):
                    pltpu.make_async_copy(kv_out.at[h], kv.at[me], kv_recv.at[me]).start()

    for h in range(2):
        j = 2 * c + h

        @pl.when(jnp.logical_not(asks_self & (j == y)))
        def _(h=h, j=j):
            remote(q_out.at[h], q_in.at[y // 2], q_send.at[h], q_recv.at[y // 2], device(j, x, z, query_core(y))).start()

        @pl.when(asks_self & (j == y))
        def _(h=h):
            pltpu.make_async_copy(q_out.at[h], q_in.at[y // 2], q_recv.at[y // 2]).start()

    to_w = remote(w_ref, weights.at[c], w_send.at[0], w_recv.at[0], partner)
    to_g = remote(gain_ref, gains.at[c], g_send.at[0], g_recv.at[0], partner)
    to_g.start()
    route()

    def to_partner(s):
        return remote(kv.at[s], kv.at[s], pair_send.at[s], pair_recv.at[s], partner)

    def arrive(column):
        def one(yy, none):
            s = yy * chips_x + column

            @pl.when(keeper & (s == me))
            def _():
                pltpu.make_async_copy(kv_out.at[0], kv.at[s], kv_recv.at[s]).wait()

            @pl.when(keeper & (s != me))
            def _():
                remote(kv_out.at[0], kv.at[s], kv_send.at[0, 1], kv_recv.at[s], partner).wait_recv()

            pl.when(keeper)(lambda: to_partner(s).start())
            return none

        lax.fori_loop(0, chips_y, one, 0)

    def handed(column):
        def one(yy, none):
            pl.when(jnp.logical_not(keeper))(lambda: to_partner(yy * chips_x + column).wait_recv())
            return none

        lax.fori_loop(0, chips_y, one, 0)

    arrive(columns[0])
    arrive(columns[1])
    for load in loads[5:]:
        load.wait()
    to_w.start()
    weights[c] = w_ref[...]
    handed(columns[0])
    handed(columns[1])

    row = lax.broadcasted_iota(jnp.int32, (CHUNK, CHUNK), 0)
    col = lax.broadcasted_iota(jnp.int32, (CHUNK, CHUNK), 1)
    after = (row > col).astype(jnp.bfloat16)

    def pair_of_blocks(slot, older, masked, shift=0):
        def part_of(place, first, length):
            return kv[older + place, pl.ds(first, length)], kv[older + place, pl.ds(rows, 16)], first // 128, length // 128

        def chunk(sources, place):
            kv_part = jnp.concatenate([s[0] for s in sources], axis=0)
            offset = jnp.concatenate(
                [s[1][s[2] + n : s[2] + n + 1, :].astype(jnp.float32) for s in sources for n in range(s[3])], axis=1
            )
            minus = (
                lax.dot_general(
                    q_wide[slot], kv_part, (((1,), (1,)), ((), ())), preferred_element_type=jnp.float32
                )
                - offset
            )
            log_part = jnp.log(1.0 + jnp.exp(-jnp.abs(minus)))
            drop = jnp.minimum(minus, 0.0) - log_part
            own_log = drop - minus
            if masked:
                q_at = lax.broadcasted_iota(jnp.int32, (rows, CHUNK), 0) + (shift - place)
                earlier = lax.broadcasted_iota(jnp.int32, (rows, CHUNK), 1) < q_at
                drop = jnp.where(earlier, drop, 0.0)
            suffix = jnp.dot(drop.astype(jnp.bfloat16), after, preferred_element_type=jnp.float32)
            within = jnp.exp(own_log + suffix)
            if masked:
                within = jnp.where(earlier, within, 0.0)
            product = jnp.dot(within.astype(jnp.bfloat16), kv_part, preferred_element_type=jnp.float32)
            now = carry[...]
            acc[...] += jnp.exp(now) * product
            carry[...] = now + (suffix[:, :1] + drop[:, :1])

        chunk([part_of(1, 128, 256)], 512)
        chunk([part_of(0, 256, 128), part_of(1, 0, 128)], 256)
        chunk([part_of(0, 0, 256)], 0)

    def query_row(slot):
        return c if slot == 0 else 3 - c

    def begin(slot):
        from_y = query_row(slot)
        asked = asks_self & (from_y == y)

        @pl.when(asked)
        def _():
            pltpu.make_async_copy(q_out.at[0], q_in.at[slot], q_recv.at[slot]).wait()

        @pl.when(jnp.logical_not(asked))
        def _():
            remote(q_out.at[0], q_in.at[slot], q_send.at[0], q_recv.at[slot], partner).wait_recv()

        folded = q_in[slot]
        q_here = jnp.concatenate([folded[:, :size], folded[:, size:]], axis=0)
        q_wide[slot] = jnp.concatenate([q_here, jnp.zeros_like(q_here)], axis=1)

        def one(yy, masked):
            acc[...] = jnp.zeros_like(acc)
            carry[...] = jnp.zeros_like(carry)
            pair_of_blocks(slot, yy * chips_x + base, masked, side * rows)
            early[slot, yy] = acc[...]
            early_carry[slot, yy] = carry[...]

        def body(yy, none):
            one(yy, False)
            return none

        one(from_y, True)
        lax.fori_loop(0, from_y, body, 0)

    def attend(slot):
        from_y = query_row(slot)
        acc[...] = jnp.zeros_like(acc)
        carry[...] = jnp.zeros_like(carry)
        newest = from_y - (1 - base // 2)

        def body(n, none):
            now = carry[...]
            acc[...] += jnp.exp(now) * early[slot, from_y - n]
            carry[...] = now + early_carry[slot, from_y - n]

            @pl.when(n <= newest)
            def _():
                pair_of_blocks(slot, (newest - n) * chips_x + other, False)

            return none

        lax.fori_loop(0, from_y + 1, body, 0)
        mixture = acc[...][:, size:]
        scaled = mixture * lax.rsqrt(jnp.mean(mixture * mixture, axis=-1, keepdims=True) + epsilon)
        scaled = scaled * gains[y // 2, pl.ds(y % 2, 1), :]
        by_owner = scaled.reshape(chips, 2, rows // (2 * chips), size)
        for p in range(2):
            att_out[slot, p] = by_owner[:, p].astype(jnp.bfloat16)
            stays = (from_y == y) & (p == c)

            @pl.when(stays)
            def _(p=p):
                pltpu.make_async_copy(att_out.at[slot, p], att_in.at[y], att_recv.at[y]).start()

            @pl.when(jnp.logical_not(stays))
            def _(p=p):
                send_att(slot, p, from_y).start()

    def send_att(slot, p, from_y):
        return remote(
            att_out.at[slot, p], att_in.at[y], att_send.at[slot, p], att_recv.at[y], device(from_y, x, z, p)
        )

    begin(1)
    arrive(columns[2])
    arrive(columns[3])
    begin(0)
    handed(columns[2])
    handed(columns[3])
    to_g.wait_recv()
    attend(1)
    attend(0)

    for j in range(chips_y):
        stayed = (j == y) & (query_core(y) == c)

        @pl.when(stayed)
        def _(j=j):
            pltpu.make_async_copy(att_out.at[0, 0], att_in.at[j], att_recv.at[j]).wait()

        @pl.when(jnp.logical_not(stayed))
        def _(j=j):
            remote(att_out.at[0, 0], att_in.at[j], att_send.at[0, 0], att_recv.at[j], partner).wait_recv()

    to_w.wait_recv()
    heads = [att_in[j].astype(jnp.float32).reshape(rows // 2, size) for j in range(chips_y)]
    merged = jnp.concatenate(heads, axis=1).astype(jnp.bfloat16)
    share = jnp.dot(merged, weights[...].reshape(2 * packed, width), preferred_element_type=jnp.float32)
    part[...] = share.reshape(part.shape)

    def from_sum(d, i, p):
        ref = ring_sum.at[d, i, :, quarter[p]]
        return remote(ref, ref, rs_send.at[d, i, p], rs_recv.at[d, i, p], ahead[d])

    for i in range(far):
        for order in range(4 if i else 2):
            for d in range(2):
                p = order if d == 0 else (order + 2) % 4
                at = ((z + (far - i)) if d == 0 else (z - (far - i) + chips)) % chips
                total = part[at, :, quarter[p]]
                if i > 1 or (i == 1 and order < 2):
                    from_sum(d, i - 1, p).wait_recv()
                    total = total + ring_sum[d, i - 1, :, quarter[p]].astype(jnp.float32)
                part_out[d, i, :, quarter[p]] = total.astype(jnp.bfloat16)
                remote(
                    part_out.at[d, i, :, quarter[p]],
                    ring_sum.at[d, i, :, quarter[p]],
                    rs_send.at[d, i, p],
                    rs_recv.at[d, i, p],
                    ahead[d],
                ).start()
    for d in range(2):
        for p in range(4):
            from_sum(d, far - 1, p).wait_recv()
    projected = part[z] + ring_sum[0, far - 1].astype(jnp.float32) + ring_sum[1, far - 1].astype(jnp.float32)
    stream = (residual_ref[...].astype(jnp.float32) + projected).astype(jnp.bfloat16)
    stream_ref[...] = stream
    wide = stream.astype(jnp.float32)
    normed_ref[...] = (
        wide * lax.rsqrt(jnp.mean(wide * wide, axis=-1, keepdims=True) + epsilon) * norm_ref[...]
    ).astype(jnp.bfloat16)

    for h in range(2):
        j = 2 * c + h

        pl.when(jnp.logical_not(j == y))(lambda h=h: to_column(h, 0).wait_send())
        for n in range(1, 4):
            to_column(h, n).wait_send()

        @pl.when(jnp.logical_not(asks_self & (j == y)))
        def _(h=h):
            remote(q_out.at[h], q_in.at[0], q_send.at[h], q_recv.at[0], partner).wait_send()

    to_w.wait_send()
    to_g.wait_send()

    def drain_pair(s, none):
        pl.when(keeper)(lambda: to_partner(s).wait_send())
        return none

    lax.fori_loop(0, sources, drain_pair, 0)
    for slot in range(2):
        from_y = c if slot == 0 else 3 - c
        for p in range(2):

            @pl.when(jnp.logical_not((from_y == y) & (p == c)))
            def _(slot=slot, p=p, from_y=from_y):
                send_att(slot, p, from_y).wait_send()

    for d in range(2):
        for i in range(far):
            for order in range(4 if i else 2):
                from_sum(d, i, order if d == 0 else (order + 2) % 4).wait_send()


def expert_part(
    chips_y, cap, loads, gate_w, up_w, down_w, stream_ref, normed_ref, select_ref, weight_ref, out_ref,
    outgoing, arrived, rows, part, partner_part, ring_sum, back, returned, hidden,
    go_send, go_recv, ag_send, ag_recv, pair_send, pair_recv, pin_send, pin_recv,
    rs_send, rs_recv, back_send, back_recv,
):
    experts, _, width = outgoing.shape
    chunks, chips, _, block, _ = rows.shape
    far, half, per = chips // 2, width // 2, experts // chunks
    me, t = lax.axis_index("sp"), lax.axis_index("tp")
    z, c = t // 2, t % 2
    chips_x = experts // chips_y
    y, x = me // chips_x, me % chips_x
    moves = sorted(
        ((dy, dx) for dy in range(chips_y) for dx in range(chips_x)),
        key=lambda move: min(move[0], chips_y - move[0]) + min(move[1], chips_x - move[1]),
    )
    to_sp = [(y + dy) % chips_y * chips_x + (x + dx) % chips_x for dy, dx in moves]
    from_sp = [(y + chips_y - dy) % chips_y * chips_x + (x + chips_x - dx) % chips_x for dy, dx in moves]
    partner = (me, 2 * z + (1 - c))
    ahead = ((me, 2 * ((z + 1) % chips) + c), (me, 2 * ((z + chips - 1) % chips) + c))
    piece = (pl.ds(0, half), pl.ds(half, half))
    quarter = [pl.ds(n * half // 2, half // 2) for n in range(4)]

    chosen = jnp.dot(select_ref[...], normed_ref[...], preferred_element_type=jnp.float32)
    outgoing[...] = chosen.reshape(experts, SLOT_ROWS, width).astype(jnp.bfloat16)
    for k in range(chunks):
        for d in range(2):
            ring_sum[k, d, 0, :, piece[1 - d]] = jnp.zeros((block, half), jnp.bfloat16)

    def go(n):
        return remote(outgoing.at[to_sp[n]], arrived.at[n], go_send.at[n], go_recv.at[n], (to_sp[n], t))

    own = pltpu.make_async_copy(outgoing.at[me], arrived.at[0], go_recv.at[0])
    own.start()
    for n in range(1, experts):
        go(n).start()

    def take_arrived(k):
        for n in range(k * per, (k + 1) * per):
            (go(n).wait_recv if n else own.wait)()
        row = lax.broadcasted_iota(jnp.int32, (block, per * SLOT_ROWS), 0)
        col = lax.broadcasted_iota(jnp.int32, (block, per * SLOT_ROWS), 1)
        pick = (col == row // cap * SLOT_ROWS + row % cap).astype(jnp.bfloat16)
        padded = arrived[pl.ds(k * per, per)].astype(jnp.float32).reshape(per * SLOT_ROWS, width)
        rows[k, z, c] = jnp.dot(
            pick, padded.astype(jnp.bfloat16), preferred_element_type=jnp.float32
        ).astype(jnp.bfloat16)

    def far_first(d, order):
        return order if d == 0 else (order + 2) % 4

    def to_partner(k, at, p):
        ref = rows.at[k, at, c, :, piece[p]]
        return remote(ref, ref, pair_send.at[k, at, p], pair_recv.at[k, at, p], partner)

    def ring_rows(k, at, d, i, p):
        ref = rows.at[k, at, c, :, quarter[p]]
        return remote(ref, ref, ag_send.at[k, d, i, p], ag_recv.at[k, d, i, p], ahead[d])

    def start_own(k):
        for order in range(4):
            for d in range(2):
                ring_rows(k, z, d, 0, far_first(d, order)).start()
        for p in range(2):
            to_partner(k, z, p).start()

    def gather_half(k, i, second):
        for order in (2, 3) if second else (0, 1):
            for d in range(2):
                p = far_first(d, order)
                at = lax.rem((z - i - 1 if d == 0 else z + i + 1) + chips, chips)
                ring_rows(k, at, d, i, p).wait_recv()

                @pl.when(i + 1 < (far - 1 if second else far))
                def _(at=at, d=d, p=p):
                    ring_rows(k, at, d, i + 1, p).start()

                if order % 2 == 1:
                    to_partner(k, at, p // 2).start()

    def gather_step(k, i):
        gather_half(k, i, False)
        pl.when(i < far - 1)(lambda: gather_half(k, i, True))

    def wait_partner_rows(k):
        def wait_one(at, none):
            for p in range(2):
                ref = rows.at[k, at, 1 - c, :, piece[p]]
                remote(ref, ref, pair_send.at[k, at, p], pair_recv.at[k, at, p], partner).wait_recv()
            return none

        lax.fori_loop(0, chips, wait_one, 0)

    group = chips // far

    def gate_and_up(k, i):
        x = rows[k, pl.ds(i * group, group)].reshape(group * 2 * block, width)
        across = (((1,), (1,)), ((), ()))
        gate = lax.dot_general(x, gate_w[...], across, preferred_element_type=jnp.float32)
        up = lax.dot_general(x, up_w[...], across, preferred_element_type=jnp.float32)
        hidden[...] = (gate / (1.0 + jnp.exp(-gate)) * up).astype(jnp.bfloat16)

    def down(k, i):
        at = pl.ds(i * group, group)
        product = jnp.dot(hidden[...], down_w[...], preferred_element_type=jnp.float32)
        part[k, at] = product.astype(jnp.bfloat16).reshape(group, 2, block, width)
        for j in range(group):
            pin(k, i * group + j).start()

    def pin(k, at):
        return remote(
            part.at[k, at, 1 - c], partner_part.at[k, at], pin_send.at[k, at], pin_recv.at[k, at], partner
        )

    def wait_pins(k):
        def wait_one(at, none):
            pin(k, at).wait_recv()
            return none

        lax.fori_loop(0, chips, wait_one, 0)

    def from_sum(k, d, i, p):
        ref = ring_sum.at[k, d, i, :, quarter[p]]
        return remote(ref, ref, rs_send.at[k, d, i, p], rs_recv.at[k, d, i, p], ahead[d])

    def sum_half(k, i, second):
        for order in (2, 3) if second else (0, 1):
            for d in range(2):
                p = far_first(d, order)
                at = lax.rem((z + (far - i) if d == 0 else z - (far - i)) + chips, chips)
                total = part[k, at, c, :, quarter[p]].astype(jnp.float32) + partner_part[
                    k, at, :, quarter[p]
                ].astype(jnp.float32)
                if isinstance(i, int):
                    assert i == 0
                else:
                    wait = from_sum(k, d, i - 1, p).wait_recv
                    if second:
                        pl.when(i > 1)(wait)
                    else:
                        wait()
                    total = total + ring_sum[k, d, i - 1, :, quarter[p]].astype(jnp.float32)
                part[k, at, c, :, quarter[p]] = total.astype(jnp.bfloat16)
                remote(
                    part.at[k, at, c, :, quarter[p]],
                    ring_sum.at[k, d, i, :, quarter[p]],
                    rs_send.at[k, d, i, p],
                    rs_recv.at[k, d, i, p],
                    ahead[d],
                ).start()

    def send_back(k):
        for p in range(4):
            for d in range(2):
                from_sum(k, d, far - 1, p).wait_recv()
        total = (
            part[k, z, c].astype(jnp.float32)
            + partner_part[k, z].astype(jnp.float32)
            + ring_sum[k, 0, far - 1].astype(jnp.float32)
            + ring_sum[k, 1, far - 1].astype(jnp.float32)
        ).astype(jnp.bfloat16)
        row = lax.broadcasted_iota(jnp.int32, (per * SLOT_ROWS, block), 0)
        col = lax.broadcasted_iota(jnp.int32, (per * SLOT_ROWS, block), 1)
        spread = ((row % SLOT_ROWS < cap) & (col == row // SLOT_ROWS * cap + row % SLOT_ROWS)).astype(jnp.bfloat16)
        back[pl.ds(k * per, per)] = (
            jnp.dot(spread, total, preferred_element_type=jnp.float32)
            .reshape(per, SLOT_ROWS, width)
            .astype(jnp.bfloat16)
        )

        for n in range(k * per, (k + 1) * per):
            if n:
                send_home(n).start()
            else:
                pltpu.make_async_copy(back.at[0], returned.at[me], back_recv.at[me]).start()

    def send_home(n):
        return remote(back.at[n], returned.at[me], back_send.at[n], back_recv.at[me], (from_sp[n], t))

    def steps(first, last, body):
        def one(i, none):
            body(i)
            return none

        lax.fori_loop(first, last, one, 0)

    take_arrived(0)
    start_own(0)
    take_arrived(1)
    steps(0, far - 1, lambda i: gather_step(0, i))
    start_own(1)
    gather_step(0, far - 1)
    for load in loads:
        load.wait()
    wait_partner_rows(0)

    def gather_and_compute(i):
        gather_half(1, i, False)
        gate_and_up(0, i)
        gather_half(1, i, True)
        down(0, i)

    steps(0, far - 1, gather_and_compute)
    gate_and_up(0, far - 1)
    down(0, far - 1)
    wait_pins(0)
    sum_half(0, 0, False)
    gather_step(1, far - 1)
    wait_partner_rows(1)

    def sum_and_compute(i):
        sum_half(0, i, False)
        gate_and_up(1, i - 1)
        sum_half(0, i, True)
        down(1, i - 1)

    steps(1, far, sum_and_compute)
    gate_and_up(1, far - 1)
    down(1, far - 1)
    wait_pins(1)
    sum_half(1, 0, False)
    send_back(0)

    def only_sum(i):
        sum_half(1, i, False)
        sum_half(1, i, True)

    steps(1, far, only_sum)
    send_back(1)

    def wait_back(e, none):
        @pl.when(e == me)
        def _():
            pltpu.make_async_copy(back.at[e], returned.at[e], back_recv.at[e]).wait()

        @pl.when(e != me)
        def _():
            remote(back.at[e], returned.at[e], back_send.at[e], back_recv.at[e], (e, t)).wait_recv()

        return none

    lax.fori_loop(0, experts, wait_back, 0)
    picked = returned[...].astype(jnp.float32).reshape(experts * SLOT_ROWS, width).astype(jnp.bfloat16)
    combined = stream_ref[...].astype(jnp.float32)
    for n in reversed(range(3)):
        combined = combined + lax.dot_general(
            weight_ref[n], picked, (((0,), (0,)), ((), ())), preferred_element_type=jnp.float32
        )
    out_ref[...] = combined.astype(jnp.bfloat16)

    for n in range(1, experts):
        go(n).wait_send()
        send_home(n).wait_send()

    def drain_pair(at, none):
        for k in range(chunks):
            for p in range(2):
                to_partner(k, at, p).wait_send()
            pin(k, at).wait_send()
        return none

    lax.fori_loop(0, chips, drain_pair, 0)

    def drain_ring(i, none):
        for k in range(chunks):
            for d in range(2):
                for order in range(4):
                    p = far_first(d, order)
                    sent, summed = ring_rows(k, 0, d, i, p).wait_send, from_sum(k, d, i, p).wait_send
                    if order < 2:
                        sent()
                        summed()
                    else:
                        pl.when(i < far - 1)(sent)
                        pl.when(i > 0)(summed)
        return none

    lax.fori_loop(0, far, drain_ring, 0)


def layer_kernel(
    chips_y, cap, q_hbm, k_hbm, v_hbm, bias_hbm, gain_hbm, w_hbm, residual_hbm, norm_hbm, choice_hbm, share_hbm,
    gate_hbm, up_hbm, down_hbm, out_ref, q, k, v, bias, gain, w, residual, norm, choice, share, gate_w, up_w, down_w,
    load_sem, stream, normed, select, weight, *scratch,
):
    sources = (q_hbm, k_hbm, v_hbm, bias_hbm, gain_hbm, w_hbm, residual_hbm, norm_hbm, choice_hbm, share_hbm)
    sources += (gate_hbm.at[0], up_hbm.at[0], down_hbm.at[0])
    places = (q, k, v, bias, gain, w, residual, norm, choice, share, gate_w, up_w, down_w)
    loads = [pltpu.make_async_copy(src, dst, load_sem.at[i]) for i, (src, dst) in enumerate(zip(sources, places))]
    for load in loads:
        load.start()

    def route():
        for load in loads[8:10]:
            load.wait()
        slots, own_rows = select.shape
        slot = lax.broadcasted_iota(jnp.int32, (slots, own_rows), 0)
        expert, place = slot // SLOT_ROWS, slot % SLOT_ROWS
        first = choice[0:1, :] == expert
        named = first | (choice[1:2, :] == expert)
        earlier = lax.broadcasted_iota(jnp.int32, (own_rows, own_rows), 0) < lax.broadcasted_iota(
            jnp.int32, (own_rows, own_rows), 1
        )
        before = jnp.dot(
            named.astype(jnp.bfloat16), earlier.astype(jnp.bfloat16), preferred_element_type=jnp.float32
        )
        chosen = named & (before.astype(jnp.int32) == place)
        select[...] = chosen.astype(jnp.bfloat16)
        rest = jnp.where(chosen, jnp.where(first, share[0:1, :], share[1:2, :]), 0.0)
        for n in range(3):
            term = rest.astype(jnp.bfloat16)
            weight[n] = term
            rest = rest - term.astype(jnp.float32)

    attention_part(
        chips_y, loads[:8], route, q, k, v, bias, gain, w, residual, norm, stream, normed, *scratch[:ATTENTION_SCRATCH]
    )
    expert_part(chips_y, cap, loads[10:], gate_w, up_w, down_w, stream, normed, select, weight, out_ref, *scratch[ATTENTION_SCRATCH:])


ATTENTION_SCRATCH = 30


def layer(
    queries, keys, values, key_bias, head_gain, out_weight, residual, norm_gain, gate_proj, up_proj, down_proj,
    expert_choice, expert_weights,
):
    rows, packed = queries.shape
    size, width, hidden = head_gain.shape[1], out_weight.shape[1], gate_proj.shape[2]
    blocks, chips, chips_y, chunks = lax.axis_size("sp"), lax.axis_size("tp") // 2, 4, 2
    chips_x, far, own = blocks // chips_y, chips // 2, residual.shape[0]
    cap = 4 * own // blocks
    block, slots = blocks // chunks * cap, blocks * SLOT_ROWS
    bf16, f32, dma = jnp.bfloat16, jnp.float32, pltpu.SemaphoreType.DMA
    arguments = (
        queries, keys, values, key_bias.T, head_gain, out_weight, residual, norm_gain.reshape(1, -1),
        expert_choice.T, expert_weights.T, gate_proj.swapaxes(1, 2), up_proj.swapaxes(1, 2), down_proj,
    )
    scratch = [pltpu.VMEM(a.shape[-2:], a.dtype) for a in arguments]
    scratch += [
        dma((len(arguments),)),
        pltpu.VMEM((own, width), bf16),
        pltpu.VMEM((own, width), bf16),
        pltpu.VMEM((slots, own), bf16),
        pltpu.VMEM((3, slots, own), bf16),
    ]
    attention_scratch = [
        pltpu.VMEM((2, rows + 16, packed), bf16),
        pltpu.VMEM((2, rows // 2, packed), bf16),
        pltpu.VMEM((blocks, rows + 16, packed), bf16),
        pltpu.VMEM((2, rows // 2, packed), bf16),
        pltpu.VMEM((2, rows, packed), bf16),
        pltpu.VMEM((2, 2, size), f32),
        pltpu.VMEM((2, packed, width), bf16),
        pltpu.VMEM((rows, packed), f32),
        pltpu.VMEM((rows, 1), f32),
        pltpu.VMEM((2, chips_y, rows, packed), f32),
        pltpu.VMEM((2, chips_y, rows, 1), f32),
        pltpu.VMEM((2, 2, chips, own, size), bf16),
        pltpu.VMEM((chips_y, chips, own, size), bf16),
        pltpu.VMEM((chips, own, width), f32),
        pltpu.VMEM((2, far, own, width), bf16),
        pltpu.VMEM((2, far, own, width), bf16),
        dma((2, 4)),
        dma((blocks,)),
        dma((2,)),
        dma((2,)),
        dma((blocks,)),
        dma((blocks,)),
        dma((1,)),
        dma((1,)),
        dma((1,)),
        dma((1,)),
        dma((2, 2)),
        dma((chips_y,)),
        dma((2, far, 4)),
        dma((2, far, 4)),
    ]
    expert_scratch = [
        pltpu.VMEM((blocks, SLOT_ROWS, width), bf16),
        pltpu.VMEM((blocks, SLOT_ROWS, width), bf16),
        pltpu.VMEM((chunks, chips, 2, block, width), bf16),
        pltpu.VMEM((chunks, chips, 2, block, width), bf16),
        pltpu.VMEM((chunks, chips, block, width), bf16),
        pltpu.VMEM((chunks, 2, far, block, width), bf16),
        pltpu.VMEM((blocks, SLOT_ROWS, width), bf16),
        pltpu.VMEM((blocks, SLOT_ROWS, width), bf16),
        pltpu.VMEM((chips // far * 2 * block, hidden), bf16),
        dma((blocks,)),
        dma((blocks,)),
        dma((chunks, 2, far, 4)),
        dma((chunks, 2, far, 4)),
        dma((chunks, chips, 2)),
        dma((chunks, chips, 2)),
        dma((chunks, chips)),
        dma((chunks, chips)),
        dma((chunks, 2, far, 4)),
        dma((chunks, 2, far, 4)),
        dma((blocks,)),
        dma((blocks,)),
    ]
    assert len(attention_scratch) == ATTENTION_SCRATCH
    return pl.pallas_call(
        functools.partial(layer_kernel, chips_y, cap),
        out_shape=jax.ShapeDtypeStruct(residual.shape, bf16),
        in_specs=[pl.BlockSpec(memory_space=pl.ANY)] * len(arguments),
        out_specs=pl.BlockSpec(memory_space=pltpu.VMEM),
        scratch_shapes=scratch + attention_scratch + expert_scratch,
        compiler_params=pltpu.CompilerParams(collective_id=1, has_side_effects=True, vmem_limit_bytes=60 << 20),
        name="layer",
    )(*arguments)


def solution(mesh):
    placed = (
        P("sp", "tp"),
        P("sp", "tp"),
        P("sp", "tp"),
        P("sp", "tp"),
        P("tp", None),
        P("tp", None),
        P(("sp", "tp"), None),
        P(),
        P("sp", None, "tp"),
        P("sp", None, "tp"),
        P("sp", "tp", None),
        P(("sp", "tp"), None),
        P(("sp", "tp"), None),
    )
    return jax.shard_map(
        layer, mesh=mesh, in_specs=placed, out_specs=P(("sp", "tp"), None), check_vma=False
    )
```

time: 154 us -> 146 us (0.948)
  Pallas kernels: 153 us -> 143 us
    pallas_call x1, Pallas kernels: 153 us -> 143 us  [layer(): pl.pallas_call(functools.partial(layer_kernel, chips_y, cap), out_shape=j...]
where the time goes in v5:
time: 146 us; the launch traced here: 145 us
  Pallas kernels  143 us (98%)
  local copies, waits for them, and re-layouts  1.54 us (1%)
    pallas_call x1, Pallas kernels, layer(): pl.pallas_call(functools.partial(layer_kernel, chips_y, cap), out_shape=j...  143 us

profile of v5, /device:TPU:24, one launch (start us, length us, event | category | flops | bytes accessed | tf_op | source)
XLA Modules:
  0.0 144.6 jit_solution(17987374785336222003)
XLA Ops:
  0.0 143.1 %layer.1 = bf16[24,2048]{1,0:T(8,128)(2,1)} custom-call(bf16[384,128]{1,0:T(8,128)(2,1)} %q_hbm.1, bf16[384,128]{1,0:T(8,128)(2,1)} %k_hbm.1, bf16[384,128]{1,0:T(8,128)(2,1)} %v_hbm.1, bf16[2,384]{1,0:T(2,128)(2,1)} %bitcast.9, f32[2,64]{1,0:T(2,128)} %gain_hbm.1, bf16[128,2048]{1,0:T(8,128)(2,1)} %w_hbm.1, bf16[24,2048]{1,0:T(8,128)(2,1)} %residual_hbm.1, ...), custom_call_target="tpu_custom_call" | custom-call | tf_op jit(solution)/shard_map/layer/pallas_call | solution.py:752
  143.1 1.5 %copy.15 = bf16[24,2048]{1,0:T(8,128)(2,1)} copy(bf16[24,2048]{1,0:T(8,128)(2,1)} %layer.1) | data formatting | bytes 196608

commit v6 on v5

--- a/solution.py
+++ b/solution.py
@@ -278,14 +278,23 @@
     to_w.wait_recv()
     heads = [att_in[j].astype(jnp.float32).reshape(rows // 2, size) for j in range(chips_y)]
     merged = jnp.concatenate(heads, axis=1).astype(jnp.bfloat16)
-    share = jnp.dot(merged, weights[...].reshape(2 * packed, width), preferred_element_type=jnp.float32)
-    part[...] = share.reshape(part.shape)
+    farthest = (z + far) % chips
+    far_heads = [att_in[j, farthest].astype(jnp.float32) for j in range(chips_y)]
+    far_merged = jnp.concatenate(far_heads, axis=1).astype(jnp.bfloat16)
+    rows_of_w = weights[...].reshape(2 * packed, width)
+    part[farthest] = jnp.dot(far_merged, rows_of_w, preferred_element_type=jnp.float32)
+
+    def rest_of_part():
+        share = jnp.dot(merged, rows_of_w, preferred_element_type=jnp.float32)
+        part[...] = share.reshape(part.shape)
 
     def from_sum(d, i, p):
         ref = ring_sum.at[d, i, :, quarter[p]]
         return remote(ref, ref, rs_send.at[d, i, p], rs_recv.at[d, i, p], ahead[d])
 
     for i in range(far):
+        if i == 1:
+            rest_of_part()
         for order in range(4 if i else 2):
             for d in range(2):
                 p = order if d == 0 else (order + 2) % 4
@@ -377,7 +386,7 @@
             ring_sum[k, d, 0, :, piece[1 - d]] = jnp.zeros((block, half), jnp.bfloat16)
 
     def go(n):
-        return remote(outgoing.at[to_sp[n]], arrived.at[n], go_send.at[n], go_recv.at[n], (to_sp[n], t))
+        return remote(outgoing.at[to_sp[n], pl.ds(0, cap)], arrived.at[n, pl.ds(0, cap)], go_send.at[n], go_recv.at[n], (to_sp[n], t))
 
     own = pltpu.make_async_copy(outgoing.at[me], arrived.at[0], go_recv.at[0])
     own.start()
@@ -524,7 +533,9 @@
                 pltpu.make_async_copy(back.at[0], returned.at[me], back_recv.at[me]).start()
 
     def send_home(n):
-        return remote(back.at[n], returned.at[me], back_send.at[n], back_recv.at[me], (from_sp[n], t))
+        return remote(
+            back.at[n, pl.ds(0, cap)], returned.at[me, pl.ds(0, cap)], back_send.at[n], back_recv.at[me], (from_sp[n], t)
+        )
 
     def steps(first, last, body):
         def one(i, none):
@@ -535,8 +546,9 @@
 
     take_arrived(0)
     start_own(0)
+    gather_step(0, 0)
     take_arrived(1)
-    steps(0, far - 1, lambda i: gather_step(0, i))
+    steps(1, far - 1, lambda i: gather_step(0, i))
     start_own(1)
     gather_step(0, far - 1)
     for load in loads:
@@ -584,7 +596,8 @@
 
         @pl.when(e != me)
         def _():
-            remote(back.at[e], returned.at[e], back_send.at[e], back_recv.at[e], (e, t)).wait_recv()
+            kept = returned.at[e, pl.ds(0, cap)]
+            remote(kept, kept, back_send.at[e], back_recv.at[e], (e, t)).wait_recv()
 
         return none
 
@@ -636,10 +649,14 @@
     sources += (gate_hbm.at[0], up_hbm.at[0], down_hbm.at[0])
     places = (q, k, v, bias, gain, w, residual, norm, choice, share, gate_w, up_w, down_w)
     loads = [pltpu.make_async_copy(src, dst, load_sem.at[i]) for i, (src, dst) in enumerate(zip(sources, places))]
-    for load in loads:
+    for load in loads[:5]:
         load.start()
+    for landing in (scratch[ATTENTION_SCRATCH + 1], scratch[ATTENTION_SCRATCH + 7]):
+        landing[...] = jnp.zeros_like(landing)
 
     def route():
+        for load in loads[5:]:
+            load.start()
         for load in loads[8:10]:
             load.wait()
         slots, own_rows = select.shape

time: 146 us -> 145 us (level)
  no operation moved by 1% of the time
where the time goes in v6:
time: 145 us; the launch traced here: 144 us
  Pallas kernels  142 us (98%)
  local copies, waits for them, and re-layouts  1.54 us (1%)
    pallas_call x1, Pallas kernels, layer(): pl.pallas_call(functools.partial(layer_kernel, chips_y, cap), out_shape=j...  142 us

profile of v6, /device:TPU:24, one launch (start us, length us, event | category | flops | bytes accessed | tf_op | source)
XLA Modules:
  0.0 143.6 jit_solution(7861738985701609487)
XLA Ops:
  0.0 142.0 %layer.1 = bf16[24,2048]{1,0:T(8,128)(2,1)} custom-call(bf16[384,128]{1,0:T(8,128)(2,1)} %q_hbm.1, bf16[384,128]{1,0:T(8,128)(2,1)} %k_hbm.1, bf16[384,128]{1,0:T(8,128)(2,1)} %v_hbm.1, bf16[2,384]{1,0:T(2,128)(2,1)} %bitcast.9, f32[2,64]{1,0:T(2,128)} %gain_hbm.1, bf16[128,2048]{1,0:T(8,128)(2,1)} %w_hbm.1, bf16[24,2048]{1,0:T(8,128)(2,1)} %residual_hbm.1, ...), custom_call_target="tpu_custom_call" | custom-call | tf_op jit(solution)/shard_map/layer/pallas_call | solution.py:769
  142.1 1.5 %copy.15 = bf16[24,2048]{1,0:T(8,128)(2,1)} copy(bf16[24,2048]{1,0:T(8,128)(2,1)} %layer.1) | data formatting | bytes 196608

commit v7 on v6

--- a/solution.py
+++ b/solution.py
@@ -254,10 +254,10 @@
             att_out.at[slot, p], att_in.at[y], att_send.at[slot, p], att_recv.at[y], device(from_y, x, z, p)
         )
 
-    begin(1)
+    begin(0)
     arrive(columns[2])
     arrive(columns[3])
-    begin(0)
+    begin(1)
     handed(columns[2])
     handed(columns[3])
     to_g.wait_recv()

time: 145 us -> 145 us (level)
  no operation moved by 1% of the time
where the time goes in v7:
time: 145 us; the launch traced here: 144 us
  Pallas kernels  142 us (98%)
  local copies, waits for them, and re-layouts  1.54 us (1%)
    pallas_call x1, Pallas kernels, layer(): pl.pallas_call(functools.partial(layer_kernel, chips_y, cap), out_shape=j...  142 us

profile of v7, /device:TPU:24, one launch (start us, length us, event | category | flops | bytes accessed | tf_op | source)
XLA Modules:
  0.0 144.0 jit_solution(14620987346922918783)
XLA Ops:
  0.0 142.4 %layer.1 = bf16[24,2048]{1,0:T(8,128)(2,1)} custom-call(bf16[384,128]{1,0:T(8,128)(2,1)} %q_hbm.1, bf16[384,128]{1,0:T(8,128)(2,1)} %k_hbm.1, bf16[384,128]{1,0:T(8,128)(2,1)} %v_hbm.1, bf16[2,384]{1,0:T(2,128)(2,1)} %bitcast.9, f32[2,64]{1,0:T(2,128)} %gain_hbm.1, bf16[128,2048]{1,0:T(8,128)(2,1)} %w_hbm.1, bf16[24,2048]{1,0:T(8,128)(2,1)} %residual_hbm.1, ...), custom_call_target="tpu_custom_call" | custom-call | tf_op jit(solution)/shard_map/layer/pallas_call | solution.py:769
  142.4 1.5 %copy.15 = bf16[24,2048]{1,0:T(8,128)(2,1)} copy(bf16[24,2048]{1,0:T(8,128)(2,1)} %layer.1) | data formatting | bytes 196608
